TPU v7x, 256 devices: a whole 4x4x8 slice. The times are simulated.
256 devices in a mesh: ep: 16 (over y, x), tp: 16 (over z, core).
Axes of the slice: x: 4, y: 4, z: 8, core: 2. Of those that a mesh axis runs over, the one named last changes fastest.
Arguments:
- q_latent: bfloat16 [16384, 512], P('ep'), may hold values from -6 to 6
- kv_latent: bfloat16 [16384, 256], P('ep'), may hold values from -6 to 6
- rope_key: bfloat16 [16384, 32], P('ep'), may hold values from -1200 to 1200
- q_gain: float32 [512], replicated, may hold values from 0.1 to 1.9
- kv_gain: float32 [256], replicated, may hold values from 0.1 to 1.9
- w_query: bfloat16 [512, 1536], P(None, 'tp'), may hold values from -0.25 to 0.25
- w_keyval: bfloat16 [256, 2048], P(None, 'tp'), may hold values from -0.375 to 0.375
- w_output: bfloat16 [1024, 2048], P(None, 'tp'), may hold values from -0.1875 to 0.1875
- moe_input: bfloat16 [8192, 2048], P('ep'), may hold values from -6 to 6
- moe_gain: float32 [2048], replicated, may hold values from 0.1 to 1.9
- routes: int32 [8192, 2], P('ep'), may hold values from 0 to 15, all different within a row; in each aligned block of 32 rows (0 to 31, 32 to 63, ...) at most 6 rows name the same one
- route_weight: float32 [8192, 2], P('ep'), may hold values from 0.25 to 2
- expert_gate: bfloat16 [16, 2048, 4096], P('ep', None, 'tp'), may hold values from -0.125 to 0.125
- expert_up: bfloat16 [16, 2048, 4096], P('ep', None, 'tp'), may hold values from -0.125 to 0.125
- expert_down: bfloat16 [16, 4096, 2048], P('ep', 'tp'), may hold values from -0.09375 to 0.09375
- shared_gate: bfloat16 [2048, 2048], P(None, 'tp'), may hold values from -0.125 to 0.125
- shared_up: bfloat16 [2048, 2048], P(None, 'tp'), may hold values from -0.125 to 0.125
- shared_down: bfloat16 [2048, 2048], P('tp'), may hold values from -0.125 to 0.125
Outputs:
- mixed: bfloat16 [16384, 2048], P('ep', 'tp')
- moe_out: bfloat16 [8192, 2048], P(('ep', 'tp'))
Inputs may be any that keep to these rules, and one draw needn't show every extreme that they name: `routes`: in each aligned block of 32 rows (the rows of one device's output) no expert is named by more than 6 rows, a bound that some block reaches. Each row names 2 different experts.
All inputs are finite; a program needn't handle non-finite values.
Results may differ from a plain program's by a relative error of at most 0.023.
Values may be sent and summed in bfloat16 or wider, within the bound.
A program may use at most 128 MiB of HBM per device.

v0:
```python
import jax
import jax.numpy as jnp
from jax import lax
from jax.sharding import PartitionSpec as P

NOPE = 64
ROPE_DIM = 32
VDIM = 64
MOE_DEV = 32


norm_eps = 1e-06
layer_eps = 1e-05
rotary_base = 10000.0
floor_value = -1e30


def rms_scale(values, gain):
    widened = values.astype(jnp.float32)
    return (
        widened * lax.rsqrt(jnp.mean(widened * widened, -1, keepdims=True) + norm_eps) * gain
    ).astype(jnp.bfloat16)


def layer_scale(values, gain):
    widened = values.astype(jnp.float32)
    centred = widened - jnp.mean(widened, -1, keepdims=True)
    return (
        centred * lax.rsqrt(jnp.mean(centred * centred, -1, keepdims=True) + layer_eps) * gain
    ).astype(jnp.bfloat16)


def rotary_tables(positions):
    halfway = ROPE_DIM // 2
    inverse = rotary_base ** (-(jnp.arange(halfway, dtype=jnp.float32) * 2.0 / ROPE_DIM))
    angles = positions.astype(jnp.float32)[:, None] * inverse[None, :]
    return (jnp.cos(angles), jnp.sin(angles))


def rotate(values, cosine_table, sine_table):
    halfway = values.shape[-1] // 2
    first_half = values[..., :halfway]
    second_half = values[..., halfway:]
    return jnp.concatenate(
        [
            first_half * cosine_table - second_half * sine_table,
            second_half * cosine_table + first_half * sine_table,
        ],
        -1,
    )


def block_stats(query_block, query_pos, keyvals, rotated_keys, key_pos):
    scale = float(NOPE + ROPE_DIM) ** (-0.5)
    scores = jnp.einsum(
        "qhd,khd->hqk",
        query_block[..., :NOPE],
        keyvals[..., :NOPE],
        preferred_element_type=jnp.float32,
    )
    scores = (
        scores
        + jnp.einsum(
            "qhd,kd->hqk", query_block[..., NOPE:], rotated_keys, preferred_element_type=jnp.float32
        )
    ) * scale
    allowed = key_pos[None, :] <= query_pos[:, None]
    scores = jnp.where(allowed[None], scores, -jnp.inf)
    block_max = jnp.max(scores, -1)
    weights = jnp.exp(scores - block_max[..., None])
    block_sum = jnp.sum(weights, -1)
    attended = jnp.einsum(
        "hqk,khd->qhd",
        weights.astype(jnp.bfloat16),
        keyvals[..., NOPE:],
        preferred_element_type=jnp.float32,
    ).astype(jnp.bfloat16)
    return (block_max.T, block_sum.T, attended)


def merge_block(carried, stats):
    running_max, running_sum, running_acc = carried
    block_max, block_sum, attended = stats
    new_max = jnp.maximum(running_max, block_max)
    old_weight = jnp.exp(running_max - new_max)
    new_weight = jnp.exp(block_max - new_max)
    return (
        new_max,
        running_sum * old_weight + block_sum * new_weight,
        running_acc * old_weight[..., None] + attended.astype(jnp.float32) * new_weight[..., None],
    )


def body(
    q_latent,
    kv_latent,
    rope_key,
    q_gain,
    kv_gain,
    w_query,
    w_keyval,
    w_output,
    moe_input,
    moe_gain,
    routes,
    route_weight,
    expert_gate,
    expert_up,
    expert_down,
    shared_gate,
    shared_up,
    shared_down,
):
    row_count = q_latent.shape[0]
    own_index = lax.axis_index("ep")
    ep_count = lax.axis_size("ep")
    tp_count = lax.axis_size("tp")
    positions = own_index * row_count + jnp.arange(row_count, dtype=jnp.int32)
    cosine_table, sine_table = rotary_tables(positions)
    q_normed = rms_scale(q_latent, q_gain)
    kv_normed = rms_scale(kv_latent, kv_gain)
    key_rotated = rotate(rope_key.astype(jnp.float32), cosine_table, sine_table).astype(
        jnp.bfloat16
    )
    heads_local = w_query.shape[1] // (NOPE + ROPE_DIM)
    projected = jnp.dot(q_normed, w_query, preferred_element_type=jnp.float32)
    projected = projected.reshape(row_count, heads_local, NOPE + ROPE_DIM)
    queries = jnp.concatenate(
        [
            projected[..., :NOPE],
            rotate(projected[..., NOPE:], cosine_table[:, None, :], sine_table[:, None, :]),
        ],
        -1,
    ).astype(jnp.bfloat16)

    def expand_keys(latent_rows):
        expanded = jnp.dot(latent_rows, w_keyval, preferred_element_type=jnp.float32).astype(
            jnp.bfloat16
        )
        return expanded.reshape(latent_rows.shape[0], heads_local, NOPE + VDIM)

    initial = (
        jnp.full((row_count, heads_local), floor_value, jnp.float32),
        jnp.zeros((row_count, heads_local), jnp.float32),
        jnp.zeros((row_count, heads_local, VDIM), jnp.float32),
    )
    carried = initial
    latent_piece = lax.all_gather(kv_normed, "ep", axis=0, tiled=True)
    rotated_piece = lax.all_gather(key_rotated, "ep", axis=0, tiled=True)
    block_count = latent_piece.shape[0] // row_count

    def visit_block(inner, offset):

        def live(current):
            latent_rows = lax.dynamic_slice_in_dim(latent_piece, offset * row_count, row_count, 0)
            rotated_rows = lax.dynamic_slice_in_dim(rotated_piece, offset * row_count, row_count, 0)
            key_pos = offset * row_count + jnp.arange(row_count, dtype=jnp.int32)
            stats = block_stats(queries, positions, expand_keys(latent_rows), rotated_rows, key_pos)
            return merge_block(current, stats)

        def skipped(current):
            return current

        return (lax.cond(offset <= own_index, live, skipped, inner), None)

    carried, unused = lax.scan(visit_block, carried, jnp.arange(block_count, dtype=jnp.int32))
    running_max, running_sum, running_acc = carried
    heads_out = (
        (running_acc / running_sum[..., None])
        .astype(jnp.bfloat16)
        .reshape(row_count, heads_local * VDIM)
    )
    mixed = jnp.dot(
        lax.all_gather(heads_out, "tp", axis=1, tiled=True),
        w_output,
        preferred_element_type=jnp.float32,
    )
    mixed = mixed.astype(jnp.bfloat16)
    width = moe_input.shape[1]
    top_count = routes.shape[1]
    local_experts = expert_gate.shape[0]
    expert_count = local_experts * ep_count
    capacity = max(2, 3 * MOE_DEV * top_count // (2 * expert_count))
    normed = layer_scale(moe_input, moe_gain)
    entries = routes.reshape(tp_count, MOE_DEV * top_count)
    onehot = (entries[..., None] == jnp.arange(expert_count, dtype=jnp.int32)).astype(jnp.int32)
    earlier = jnp.cumsum(onehot, 1) - onehot
    rank_in = jnp.sum(earlier * onehot, -1)
    block_ids = jnp.arange(tp_count, dtype=jnp.int32)[:, None]
    slot_of = ((entries * tp_count + block_ids) * capacity + rank_in).reshape(-1, top_count)
    token_ids = jnp.arange(tp_count * MOE_DEV * top_count, dtype=jnp.int32) // top_count
    slot_token = (
        jnp.full((expert_count * tp_count * capacity,), -1, jnp.int32)
        .at[slot_of.reshape(-1)]
        .set(token_ids)
    )
    outgoing = jnp.where(
        (slot_token >= 0)[:, None], normed[jnp.maximum(slot_token, 0)], jnp.zeros((), jnp.bfloat16)
    )
    outgoing = outgoing.reshape(ep_count, local_experts, tp_count, capacity, width)
    arrived = lax.all_to_all(outgoing, "ep", split_axis=0, concat_axis=0, tiled=True)
    slot_rows = arrived.shape[3]
    inputs = arrived[:, 0].reshape(-1, width)
    hidden = jax.nn.silu(jnp.dot(inputs, expert_gate[0], preferred_element_type=jnp.float32))
    hidden = (hidden * jnp.dot(inputs, expert_up[0], preferred_element_type=jnp.float32)).astype(
        jnp.bfloat16
    )
    output = jnp.dot(hidden, expert_down[0], preferred_element_type=jnp.float32)
    results = [output.astype(jnp.bfloat16).reshape(ep_count, tp_count, slot_rows, width)]
    partial_value = jnp.stack(results, 1)
    shared_hidden = jax.nn.silu(jnp.dot(normed, shared_gate, preferred_element_type=jnp.float32))
    shared_hidden = (
        shared_hidden * jnp.dot(normed, shared_up, preferred_element_type=jnp.float32)
    ).astype(jnp.bfloat16)
    shared_part = jnp.dot(shared_hidden, shared_down, preferred_element_type=jnp.float32).astype(
        jnp.bfloat16
    )
    slot_total, shared_total = (
        lax.psum_scatter(
            partial_value.astype(jnp.float32).astype(jnp.bfloat16),
            "tp",
            scatter_dimension=2,
            tiled=True,
        ).astype(jnp.float32),
        lax.psum_scatter(
            shared_part.astype(jnp.float32)
            .reshape(1, 1, tp_count, MOE_DEV, width)
            .astype(jnp.bfloat16),
            "tp",
            scatter_dimension=2,
            tiled=True,
        ).astype(jnp.float32),
    )
    arrived_sums = lax.all_to_all(
        slot_total.astype(jnp.bfloat16), "ep", split_axis=0, concat_axis=0, tiled=True
    ).astype(slot_total.dtype)
    own_block = lax.axis_index("tp")
    own_entries = lax.dynamic_slice_in_dim(routes, own_block * MOE_DEV, MOE_DEV, 0)
    own_rank = lax.dynamic_slice_in_dim(
        rank_in.reshape(-1, top_count), own_block * MOE_DEV, MOE_DEV, 0
    )
    own_weight = lax.dynamic_slice_in_dim(route_weight, own_block * MOE_DEV, MOE_DEV, 0)
    picked = arrived_sums.reshape(-1, width)[own_entries * capacity + own_rank]
    moe_out = (
        jnp.sum(own_weight[..., None] * picked, 1) + shared_total.reshape(MOE_DEV, width)
    ).astype(jnp.bfloat16)
    return (mixed, moe_out)


def solution(mesh):
    in_specs = (
        P("ep", None),
        P("ep", None),
        P("ep", None),
        P(),
        P(),
        P(None, "tp"),
        P(None, "tp"),
        P(None, "tp"),
        P("ep", None),
        P(),
        P("ep", None),
        P("ep", None),
        P("ep", None, "tp"),
        P("ep", None, "tp"),
        P("ep", "tp", None),
        P(None, "tp"),
        P(None, "tp"),
        P("tp", None),
    )
    out_specs = (P("ep", "tp"), P(("ep", "tp"), None))
    return jax.shard_map(body, mesh=mesh, in_specs=in_specs, out_specs=out_specs, check_vma=False)
```

profile of v0, /device:TPU:27, one launch (start us, length us, event | category | flops | bytes accessed | tf_op | source)
XLA Modules:
  0.0 394.8 jit_solution(12056889168030014278)
XLA Ops:
  11.4 2.0 fusion.55
  19.0 4.5 %scatter_custom_fusion = s32[1536]{0:T(1024)S(1)} fusion(s32[1024]{0:T(1024)S(1)} %bitcast.106, s32[1024]{0:T(1024)S(1)} %add_select_fusion, s32[]{:T(128)} %constant.89.clone.1), kind=kCustom, calls=%fused_computation.123 | custom fusion | bytes 6148 | tf_op jit(solution)/shard_map/scatter | solution.py:195
  25.8 7.1 %gather_fusion = bf16[1536,2048]{1,0:T(8,128)(2,1)} fusion(bf16[512,2048]{1,0:T(8,128)(2,1)S(1)} %fusion.42, s32[2048]{0:T(1024)S(1)} %pad_clamp_fusion), kind=kCustom, calls=%fused_computation | custom fusion | bytes 12589056 | tf_op jit(solution)/shard_map/gather | solution.py:198
  32.9 11.0 %gather.9 = bf16[16,1,16,6,2048]{4,3,2,0,1:T(8,128)(2,1)} reshape(bf16[1536,2048]{1,0:T(8,128)(2,1)} %gather_fusion) | data formatting | bytes 12582912 | tf_op jit(solution)/shard_map/gather | solution.py:198
  44.0 7.5 %broadcast_select_fusion = bf16[16,1,16,6,2048]{4,3,2,0,1:T(8,128)(2,1)} fusion(bf16[16,1,16,6,2048]{4,3,2,0,1:T(8,128)(2,1)} %gather.9, pred[16,16,6]{2,1,0:T(8,128)(4,1)S(1)} %broadcast_in_dim.36), kind=kLoop, calls=%fused_computation.37 | loop fusion | flops 3145728 | bytes 12584448 | tf_op jit(solution)/shard_map/jit(_where)/select_n | solution.py:197
  51.5 7.6 %copy.36 = bf16[16,1,16,6,2048]{4,2,3,1,0:T(8,128)(2,1)S(1)} copy(bf16[16,1,16,6,2048]{4,3,2,0,1:T(8,128)(2,1)} %broadcast_select_fusion) | data formatting | bytes 12582912 | tf_op jit(solution)/shard_map/jit(_where)/select_n | solution.py:197
  59.1 84.7 %all_to_all.10 = bf16[16,1,16,6,2048]{4,2,3,1,0:T(8,128)(2,1)} all-to-all(bf16[16,1,16,6,2048]{4,2,3,1,0:T(8,128)(2,1)S(1)} %copy.36), channel_id=1, replica_groups=mesh['ep'=16,'tp'=16] {'ep'}, dimensions={0} | all-to-all | bytes 12582912 | tf_op jit(solution)/shard_map/all_to_all | solution.py:201
  143.7 11.2 %copy.37 = bf16[16,1,16,6,2048]{4,3,2,0,1:T(8,128)(2,1)} copy(bf16[16,1,16,6,2048]{4,2,3,1,0:T(8,128)(2,1)} %all_to_all.10) | data formatting | bytes 12582912 | tf_op jit(solution)/shard_map/all_to_all | solution.py:201
  154.9 11.2 %reshape_squeeze.3 = bf16[1536,2048]{1,0:T(8,128)(2,1)} reshape(bf16[16,1,16,6,2048]{4,3,2,0,1:T(8,128)(2,1)} %copy.37) | data formatting | bytes 12582912 | tf_op jit(solution)/shard_map/reshape;squeeze | solution.py:203
  166.1 6.2 %fusion.60 = f32[1536,256]{1,0:T(8,128)} fusion(bf16[1536,2048]{1,0:T(8,128)(2,1)} %reshape_squeeze.3, bf16[1,2048,256]{2,1,0:T(8,128)(2,1)} %param.34), kind=kOutput, calls=%fused_computation.67 | convolution fusion | flops 1610612736 | bytes 8912896 | tf_op jit(solution)/shard_map/dot_general | solution.py:204
  172.3 12.8 %convolution_convert_fusion.1 = bf16[1536,2048]{1,0:T(8,128)(2,1)} fusion(bf16[1536,2048]{1,0:T(8,128)(2,1)} %reshape_squeeze.3, f32[1536,256]{1,0:T(8,128)} %fusion.60, bf16[1,256,2048]{2,1,0:T(8,128)(2,1)S(1)} %copy-done, bf16[1,2048,256]{2,1,0:T(8,128)(2,1)} %param.35), kind=kOutput, calls=%fused_computation.38 | convolution fusion | flops 3226730496 | bytes 16252928 | tf_op jit(solution)/shard_map/dot_general | solution.py:208
  185.1 11.2 %stack_reshape.3 = bf16[16,1,16,6,2048]{4,3,2,0,1:T(8,128)(2,1)} reshape(bf16[1536,2048]{1,0:T(8,128)(2,1)} %convolution_convert_fusion.1) | data formatting | bytes 12582912 | tf_op jit(solution)/shard_map/stack;reshape | solution.py:210
  196.3 10.8 %copy.38 = bf16[16,1,16,6,2048]{4,0,3,1,2:T(8,128)(2,1)} copy(bf16[16,1,16,6,2048]{4,3,2,0,1:T(8,128)(2,1)} %stack_reshape.3) | data formatting | bytes 12582912 | tf_op jit(solution)/shard_map/stack;reshape | solution.py:210
  209.5 5.0 %convolution_convert_fusion.2 = bf16[512,2048]{1,0:T(8,128)(2,1)} fusion(bf16[128,2048]{1,0:T(8,128)(2,1)} %param.39, bf16[512,2048]{1,0:T(8,128)(2,1)S(1)} %fusion.42, bf16[2048,128]{1,0:T(8,128)(2,1)} %param.38, f32[512,128]{1,0:T(8,128)} %fusion.101), kind=kOutput, calls=%fused_computation.46 | convolution fusion | flops 538312704 | bytes 5505024 | tf_op jit(solution)/shard_map/dot_general | solution.py:215
  217.1 4.6 %copy.30 = bf16[16384,32]{1,0:T(8,128)(2,1)} copy(bf16[16384,32]{0,1:T(8,128)(2,1)} %all-gather.7.cloned.1.call-done) | data formatting | bytes 2097152
  221.8 106.5 %while.15 = (s32[]{:T(128)}, f32[1024,1]{0,1:T(1,128)S(1)}, f32[1024,1]{0,1:T(1,128)S(1)}, f32[1024,1,64]{0,2,1:T(8,128)S(1)}, s32[16]{0:T(128)S(1)}, /*index=5*...) while((s32[]{:T(128)}, f32[1024,1]{0,1:T(1,128)S(1)}, ...), condition=%wide.region_7.8_spmd.clone, body=%wide.region_2.7_spmd.clone.sunk | while | flops 412555264 | bytes 23150940 | solution.py:166
  223.1 6.1 %conditional.3 = ((f32[1024,1]{0,1:T(1,128)S(1)}, f32[1024,1]{0,1:T(1,128)S(1)}, f32[1024,1,64]{0,2,1:T(8,128)S(1)})) conditional(s32[]{:T(128)} %convert_element_type.204, (f32[1024,1]{0,1:T(1,128)S(1)}, f32[1024,1]{0,1:T(1,128)S(1)}, f32[1024,1,64]{0,2,1:T(8,128)S(1)}) %tuple.45, (s32[]{:T(128)}, s32[]{:T(128)}, bf16[16384,256]{1,0:T(8,128)(2,1)}, ...), branch_computations={%region_3.3_spmd, %region_4.6_spmd} | conditional | flops 412555264 | bytes 23146590 | solution.py:164
  225.9 1.9 fusion.100
  230.5 6.2 %conditional.3 = ((f32[1024,1]{0,1:T(1,128)S(1)}, f32[1024,1]{0,1:T(1,128)S(1)}, f32[1024,1,64]{0,2,1:T(8,128)S(1)})) conditional(s32[]{:T(128)} %convert_element_type.204, (f32[1024,1]{0,1:T(1,128)S(1)}, f32[1024,1]{0,1:T(1,128)S(1)}, f32[1024,1,64]{0,2,1:T(8,128)S(1)}) %tuple.45, (s32[]{:T(128)}, s32[]{:T(128)}, bf16[16384,256]{1,0:T(8,128)(2,1)}, ...), branch_computations={%region_3.3_spmd, %region_4.6_spmd} | conditional | flops 412555264 | bytes 23146590 | solution.py:164
  233.3 1.9 fusion.100
  237.9 6.1 %conditional.3 = ((f32[1024,1]{0,1:T(1,128)S(1)}, f32[1024,1]{0,1:T(1,128)S(1)}, f32[1024,1,64]{0,2,1:T(8,128)S(1)})) conditional(s32[]{:T(128)} %convert_element_type.204, (f32[1024,1]{0,1:T(1,128)S(1)}, f32[1024,1]{0,1:T(1,128)S(1)}, f32[1024,1,64]{0,2,1:T(8,128)S(1)}) %tuple.45, (s32[]{:T(128)}, s32[]{:T(128)}, bf16[16384,256]{1,0:T(8,128)(2,1)}, ...), branch_computations={%region_3.3_spmd, %region_4.6_spmd} | conditional | flops 412555264 | bytes 23146590 | solution.py:164
  240.7 1.9 fusion.100
  245.4 6.1 %conditional.3 = ((f32[1024,1]{0,1:T(1,128)S(1)}, f32[1024,1]{0,1:T(1,128)S(1)}, f32[1024,1,64]{0,2,1:T(8,128)S(1)})) conditional(s32[]{:T(128)} %convert_element_type.204, (f32[1024,1]{0,1:T(1,128)S(1)}, f32[1024,1]{0,1:T(1,128)S(1)}, f32[1024,1,64]{0,2,1:T(8,128)S(1)}) %tuple.45, (s32[]{:T(128)}, s32[]{:T(128)}, bf16[16384,256]{1,0:T(8,128)(2,1)}, ...), branch_computations={%region_3.3_spmd, %region_4.6_spmd} | conditional | flops 412555264 | bytes 23146590 | solution.py:164
  248.1 1.9 fusion.100
  252.8 6.1 %conditional.3 = ((f32[1024,1]{0,1:T(1,128)S(1)}, f32[1024,1]{0,1:T(1,128)S(1)}, f32[1024,1,64]{0,2,1:T(8,128)S(1)})) conditional(s32[]{:T(128)} %convert_element_type.204, (f32[1024,1]{0,1:T(1,128)S(1)}, f32[1024,1]{0,1:T(1,128)S(1)}, f32[1024,1,64]{0,2,1:T(8,128)S(1)}) %tuple.45, (s32[]{:T(128)}, s32[]{:T(128)}, bf16[16384,256]{1,0:T(8,128)(2,1)}, ...), branch_computations={%region_3.3_spmd, %region_4.6_spmd} | conditional | flops 412555264 | bytes 23146590 | solution.py:164
  255.6 1.9 fusion.100
  260.2 6.1 %conditional.3 = ((f32[1024,1]{0,1:T(1,128)S(1)}, f32[1024,1]{0,1:T(1,128)S(1)}, f32[1024,1,64]{0,2,1:T(8,128)S(1)})) conditional(s32[]{:T(128)} %convert_element_type.204, (f32[1024,1]{0,1:T(1,128)S(1)}, f32[1024,1]{0,1:T(1,128)S(1)}, f32[1024,1,64]{0,2,1:T(8,128)S(1)}) %tuple.45, (s32[]{:T(128)}, s32[]{:T(128)}, bf16[16384,256]{1,0:T(8,128)(2,1)}, ...), branch_computations={%region_3.3_spmd, %region_4.6_spmd} | conditional | flops 412555264 | bytes 23146590 | solution.py:164
  263.0 1.9 fusion.100
  267.6 6.1 %conditional.3 = ((f32[1024,1]{0,1:T(1,128)S(1)}, f32[1024,1]{0,1:T(1,128)S(1)}, f32[1024,1,64]{0,2,1:T(8,128)S(1)})) conditional(s32[]{:T(128)} %convert_element_type.204, (f32[1024,1]{0,1:T(1,128)S(1)}, f32[1024,1]{0,1:T(1,128)S(1)}, f32[1024,1,64]{0,2,1:T(8,128)S(1)}) %tuple.45, (s32[]{:T(128)}, s32[]{:T(128)}, bf16[16384,256]{1,0:T(8,128)(2,1)}, ...), branch_computations={%region_3.3_spmd, %region_4.6_spmd} | conditional | flops 412555264 | bytes 23146590 | solution.py:164
  270.4 1.9 fusion.100
  275.1 6.1 %conditional.3 = ((f32[1024,1]{0,1:T(1,128)S(1)}, f32[1024,1]{0,1:T(1,128)S(1)}, f32[1024,1,64]{0,2,1:T(8,128)S(1)})) conditional(s32[]{:T(128)} %convert_element_type.204, (f32[1024,1]{0,1:T(1,128)S(1)}, f32[1024,1]{0,1:T(1,128)S(1)}, f32[1024,1,64]{0,2,1:T(8,128)S(1)}) %tuple.45, (s32[]{:T(128)}, s32[]{:T(128)}, bf16[16384,256]{1,0:T(8,128)(2,1)}, ...), branch_computations={%region_3.3_spmd, %region_4.6_spmd} | conditional | flops 412555264 | bytes 23146590 | solution.py:164
  282.5 6.1 %conditional.3 = ((f32[1024,1]{0,1:T(1,128)S(1)}, f32[1024,1]{0,1:T(1,128)S(1)}, f32[1024,1,64]{0,2,1:T(8,128)S(1)})) conditional(s32[]{:T(128)} %convert_element_type.204, (f32[1024,1]{0,1:T(1,128)S(1)}, f32[1024,1]{0,1:T(1,128)S(1)}, f32[1024,1,64]{0,2,1:T(8,128)S(1)}) %tuple.45, (s32[]{:T(128)}, s32[]{:T(128)}, bf16[16384,256]{1,0:T(8,128)(2,1)}, ...), branch_computations={%region_3.3_spmd, %region_4.6_spmd} | conditional | flops 412555264 | bytes 23146590 | solution.py:164
  285.3 1.9 fusion.100
  289.9 6.1 %conditional.3 = ((f32[1024,1]{0,1:T(1,128)S(1)}, f32[1024,1]{0,1:T(1,128)S(1)}, f32[1024,1,64]{0,2,1:T(8,128)S(1)})) conditional(s32[]{:T(128)} %convert_element_type.204, (f32[1024,1]{0,1:T(1,128)S(1)}, f32[1024,1]{0,1:T(1,128)S(1)}, f32[1024,1,64]{0,2,1:T(8,128)S(1)}) %tuple.45, (s32[]{:T(128)}, s32[]{:T(128)}, bf16[16384,256]{1,0:T(8,128)(2,1)}, ...), branch_computations={%region_3.3_spmd, %region_4.6_spmd} | conditional | flops 412555264 | bytes 23146590 | solution.py:164
  292.7 1.9 fusion.100
  297.3 6.2 %conditional.3 = ((f32[1024,1]{0,1:T(1,128)S(1)}, f32[1024,1]{0,1:T(1,128)S(1)}, f32[1024,1,64]{0,2,1:T(8,128)S(1)})) conditional(s32[]{:T(128)} %convert_element_type.204, (f32[1024,1]{0,1:T(1,128)S(1)}, f32[1024,1]{0,1:T(1,128)S(1)}, f32[1024,1,64]{0,2,1:T(8,128)S(1)}) %tuple.45, (s32[]{:T(128)}, s32[]{:T(128)}, bf16[16384,256]{1,0:T(8,128)(2,1)}, ...), branch_computations={%region_3.3_spmd, %region_4.6_spmd} | conditional | flops 412555264 | bytes 23146590 | solution.py:164
  300.1 1.9 fusion.100
  304.7 6.1 %conditional.3 = ((f32[1024,1]{0,1:T(1,128)S(1)}, f32[1024,1]{0,1:T(1,128)S(1)}, f32[1024,1,64]{0,2,1:T(8,128)S(1)})) conditional(s32[]{:T(128)} %convert_element_type.204, (f32[1024,1]{0,1:T(1,128)S(1)}, f32[1024,1]{0,1:T(1,128)S(1)}, f32[1024,1,64]{0,2,1:T(8,128)S(1)}) %tuple.45, (s32[]{:T(128)}, s32[]{:T(128)}, bf16[16384,256]{1,0:T(8,128)(2,1)}, ...), branch_computations={%region_3.3_spmd, %region_4.6_spmd} | conditional | flops 412555264 | bytes 23146590 | solution.py:164
  307.5 1.9 fusion.100
  312.2 6.1 %conditional.3 = ((f32[1024,1]{0,1:T(1,128)S(1)}, f32[1024,1]{0,1:T(1,128)S(1)}, f32[1024,1,64]{0,2,1:T(8,128)S(1)})) conditional(s32[]{:T(128)} %convert_element_type.204, (f32[1024,1]{0,1:T(1,128)S(1)}, f32[1024,1]{0,1:T(1,128)S(1)}, f32[1024,1,64]{0,2,1:T(8,128)S(1)}) %tuple.45, (s32[]{:T(128)}, s32[]{:T(128)}, bf16[16384,256]{1,0:T(8,128)(2,1)}, ...), branch_computations={%region_3.3_spmd, %region_4.6_spmd} | conditional | flops 412555264 | bytes 23146590 | solution.py:164
  314.9 1.9 fusion.100
  319.6 6.2 %conditional.3 = ((f32[1024,1]{0,1:T(1,128)S(1)}, f32[1024,1]{0,1:T(1,128)S(1)}, f32[1024,1,64]{0,2,1:T(8,128)S(1)})) conditional(s32[]{:T(128)} %convert_element_type.204, (f32[1024,1]{0,1:T(1,128)S(1)}, f32[1024,1]{0,1:T(1,128)S(1)}, f32[1024,1,64]{0,2,1:T(8,128)S(1)}) %tuple.45, (s32[]{:T(128)}, s32[]{:T(128)}, bf16[16384,256]{1,0:T(8,128)(2,1)}, ...), branch_computations={%region_3.3_spmd, %region_4.6_spmd} | conditional | flops 412555264 | bytes 23146590 | solution.py:164
  322.4 1.9 fusion.100
  329.1 2.0 copy.39
  331.1 18.0 %all-to-all-start.1 = ((bf16[16,1,1,6,2048]{4,3,2,1,0:T(8,128)(2,1)}), bf16[16,1,1,6,2048]{4,3,2,1,0:T(8,128)(2,1)S(1)}, u32[]{:S(2)}, u32[]{:S(2)}) async-start(bf16[16,1,1,6,2048]{4,3,2,1,0:T(8,128)(2,1)} %copy.39), calls=%async_computation.2 | async-start | bytes 1048576 | tf_op jit(solution)/shard_map/all_to_all | solution.py:234
  350.3 5.7 %all-to-all-done.1 = bf16[16,1,1,6,2048]{4,3,2,1,0:T(8,128)(2,1)S(1)} async-done(((bf16[16,1,1,6,2048]{4,3,2,1,0:T(8,128)(2,1)}), bf16[16,1,1,6,2048]{4,3,2,1,0:T(8,128)(2,1)S(1)}, u32[]{:S(2)}, u32[]{:S(2)}) %all-to-all-start.1) | async-done | bytes 393248 | tf_op jit(solution)/shard_map/all_to_all | solution.py:234
  359.6 24.0 %all-gather.9.cloned.1.call-done = bf16[1024,1,1024]{0,2,1:T(8,128)(2,1)} async-done(((bf16[1024,1,64]{0,2,1:T(8,128)(2,1)}), bf16[1024,1,1024]{0,2,1:T(8,128)(2,1)}) %all-gather.9.cloned.1.call-update) | async-done | bytes 2097168 | tf_op jit(solution)/shard_map/all_gather | solution.py:174
  383.7 3.1 fusion.49
  (205 shorter events, 82.9 us)
Async XLA Ops:
  8.0 164.3 %copy-start = (bf16[1,256,2048]{2,1,0:T(8,128)(2,1)S(1)}, bf16[1,256,2048]{2,1,0:T(8,128)(2,1)}, u32[]{:S(2)}) copy-start(bf16[1,256,2048]{2,1,0:T(8,128)(2,1)} %param.36) | copy-start | bytes 3145732
  8.0 15.5 %copy-start.2 = (bf16[512,2048]{1,0:T(8,128)(2,1)S(1)}, bf16[512,2048]{1,0:T(8,128)(2,1)}, u32[]{:S(2)}) copy-start(bf16[512,2048]{1,0:T(8,128)(2,1)} %param.30) | copy-start | bytes 6291460
  8.0 16.6 %copy-start.8 = (f32[2048]{0:T(1024)S(1)}, f32[2048]{0:T(1024)}, u32[]{:S(2)}) copy-start(f32[2048]{0:T(1024)} %param.31) | copy-start | bytes 24580
  8.0 209.1 %all-gather.7.cloned.1.call-start = ((), (), s32[]{:S(2)}) async-start(), calls=%async_computation.5 | async-start | bytes 1114112 | tf_op jit(solution)/shard_map/all_gather | solution.py:149
  10.1 211.7 %all-gather.5.cloned.1.call-start = ((), (), s32[]{:S(2)}) async-start(), calls=%async_computation.4 | async-start | bytes 8912896 | tf_op jit(solution)/shard_map/all_gather | solution.py:148
  13.5 315.6 %reduce-scatter.3.cloned.1.call-start = ((), (), s32[]{:S(2)}) async-start(), calls=%async_computation.6 | async-start | bytes 6684672 | tf_op jit(solution)/shard_map/reduce_scatter | solution.py:219
  23.5 1.6 copy-start.3
  207.0 1.0 copy-start.6
  207.1 151.0 %reduce-scatter.5.cloned.1.call-start = ((), (), s32[]{:S(2)}) async-start(), calls=%async_computation.7 | async-start | bytes 2228224 | tf_op jit(solution)/shard_map/reduce_scatter | solution.py:225
  209.5 5.1 %copy-start.5 = (bf16[1024,512]{1,0:T(8,128)(2,1)S(1)}, bf16[1024,512]{1,0:T(8,128)(2,1)}, u32[]{:S(2)}) copy-start(bf16[1024,512]{1,0:T(8,128)(2,1)} %param.22) | copy-start | bytes 3145732
  209.5 5.4 %copy-start.9 = (f32[512]{0:T(512)S(1)}, f32[512]{0:T(512)}, u32[]{:S(2)}) copy-start(f32[512]{0:T(512)} %param.25) | copy-start | bytes 6148
  214.5 169.1 %all-gather.9.cloned.1.call-start = ((), (), s32[]{:S(2)}) async-start(), calls=%async_computation.8 | async-start | bytes 2228224 | tf_op jit(solution)/shard_map/all_gather | solution.py:174
  214.9 6.9 %copy-start.4 = (bf16[256,128]{1,0:T(8,128)(2,1)S(1)}, bf16[256,128]{1,0:T(8,128)(2,1)}, u32[]{:S(2)}) copy-start(bf16[256,128]{1,0:T(8,128)(2,1)} %param.28) | copy-start | bytes 196612
  331.1 25.0 %all-to-all-start.1 = ((bf16[16,1,1,6,2048]{4,3,2,1,0:T(8,128)(2,1)}), bf16[16,1,1,6,2048]{4,3,2,1,0:T(8,128)(2,1)S(1)}, u32[]{:S(2)}, u32[]{:S(2)}) async-start(bf16[16,1,1,6,2048]{4,3,2,1,0:T(8,128)(2,1)} %copy.39), calls=%async_computation.2 | async-start | bytes 1048576 | tf_op jit(solution)/shard_map/all_to_all | solution.py:234
  350.3 33.3 %copy-start.7 = (bf16[1024,128]{1,0:T(8,128)(2,1)S(1)}, bf16[1024,128]{1,0:T(8,128)(2,1)}, u32[]{:S(2)}) copy-start(bf16[1024,128]{1,0:T(8,128)(2,1)} %param.29) | copy-start | bytes 786436
  356.2 30.5 %copy-start.1 = (bf16[1,256,2048]{2,1,0:T(8,128)(2,1)S(1)}, bf16[1,256,2048]{2,1,0:T(8,128)(2,1)}, u32[]{:S(2)}) copy-start(bf16[1,256,2048]{2,1,0:T(8,128)(2,1)} %param.36) | copy-start | bytes 3145732
Sparse Core Ops, SparseCore 0:
  11.9 46.8 all-gather.6
  61.2 131.3 all-gather.4
Sparse Core Ops, SparseCore 1:
  207.2 66.8 reduce-scatter.2
  276.4 58.8 reduce-scatter.4
  337.6 46.0 all-gather.8
where the time goes:
time: 402 us; the launch traced here: 395 us
  local copies, waits for them, and re-layouts  97.8 us (24%)
  matrix products  97.2 us (24%)
  blocking collectives  84.7 us (21%)
  waiting for transfers between devices  29.9 us (7%)
  other arithmetic  29.5 us (7%)
  loops' own time  20.9 us (5%)
  starting transfers between devices  18.2 us (5%)
  between operations  16.5 us (4%)
    all_to_all x1, blocking collectives, body(): lax.all_to_all(outgoing, 'ep', split_axis=0, concat_axis=0, tiled=True)  84.7 us
    dot_general x14, matrix products, block_stats(): jnp.einsum('qhd,kd->hqk', query_block[..., NOPE:], rotated_keys, preferre...  26.4 us
    all_gather x1, waiting for transfers between devices, body(): lax.all_gather(heads_out, 'tp', axis=1, tiled=True)  24 us
    another operation x2, local copies, waits for them, and re-layouts, body(): partial_value = jnp.stack(results, 1)  21.9 us
    dot_general x14, matrix products, expand_keys(): jnp.dot(latent_rows, w_keyval, preferred_element_type=jnp.float32)  18.9 us
    gather x2, local copies, waits for them, and re-layouts, body(): normed[jnp.maximum(slot_token, 0)]  18 us
    all_to_all x1, starting transfers between devices, body(): lax.all_to_all(slot_total.astype(jnp.bfloat16), 'ep', split_axis=0, conca...  18 us
    dot_general x1, matrix products, body(): output = jnp.dot(hidden, expert_down[0], preferred_element_type=jnp.float32)  12.8 us
  transfers between devices with their start and end apart: 6, of which 2 were waited for; matrix products, arithmetic and copies ran while one was open for 55% of the time, Pallas kernels for 0%

commit v1 on v0

v1 whole, which is shorter than its diff:
```python
import functools

import jax
import jax.numpy as jnp
from jax import lax
from jax.experimental import pallas as pl
from jax.experimental.pallas import tpu as pltpu
from jax.sharding import PartitionSpec as P

NOPE = 64
ROPE_DIM = 32
VDIM = 64
MOE_DEV = 32
CAP = 6
PAD = 8

norm_eps = 1e-06
layer_eps = 1e-05
rotary_base = 10000.0
floor_value = -1e30
QTILE = 256
LOG2E = 1.4426950408889634


def rms_scale(values, gain):
    widened = values.astype(jnp.float32)
    return (
        widened * lax.rsqrt(jnp.mean(widened * widened, -1, keepdims=True) + norm_eps) * gain
    ).astype(jnp.bfloat16)


def layer_scale(values, gain):
    widened = values.astype(jnp.float32)
    centred = widened - jnp.mean(widened, -1, keepdims=True)
    return (
        centred * lax.rsqrt(jnp.mean(centred * centred, -1, keepdims=True) + layer_eps) * gain
    ).astype(jnp.bfloat16)


def rotary_tables(positions):
    halfway = ROPE_DIM // 2
    inverse = rotary_base ** (-(jnp.arange(halfway, dtype=jnp.float32) * 2.0 / ROPE_DIM))
    angles = positions.astype(jnp.float32)[None, :] * inverse[:, None]
    return (jnp.cos(angles), jnp.sin(angles))


def rotate_rows(values, cosine_table, sine_table):
    halfway = values.shape[0] // 2
    first_half = values[:halfway]
    second_half = values[halfway:]
    return jnp.concatenate(
        [
            first_half * cosine_table - second_half * sine_table,
            second_half * cosine_table + first_half * sine_table,
        ],
        0,
    )


def attention_kernel(own_ref, q_ref, kv_ref, out_ref, m_ref, l_ref, acc_ref):
    block = pl.program_id(0)
    own = own_ref[0]
    width = q_ref.shape[1]
    score_rows = NOPE + ROPE_DIM
    scale = float(score_rows) ** (-0.5) * LOG2E

    @pl.when(block == 0)
    def _():
        m_ref[...] = jnp.full_like(m_ref, floor_value)
        l_ref[...] = jnp.zeros_like(l_ref)
        acc_ref[...] = jnp.zeros_like(acc_ref)

    def visit(tile, key_count, masked):
        cols = pl.ds(tile * QTILE, QTILE)
        scores = lax.dot_general(
            kv_ref[0:score_rows, 0:key_count],
            q_ref[:, cols],
            (((0,), (0,)), ((), ())),
            preferred_element_type=jnp.float32,
        )
        if masked:
            key_at = lax.broadcasted_iota(jnp.int32, scores.shape, 0)
            query_at = tile * QTILE + lax.broadcasted_iota(jnp.int32, scores.shape, 1)
            scores = jnp.where(key_at <= query_at, scores, floor_value)
        old_max = m_ref[:, cols]
        new_max = jnp.maximum(old_max, jnp.max(scores, 0, keepdims=True))
        weights = jnp.exp2((scores - new_max) * scale)
        fade = jnp.exp2((old_max - new_max) * scale)
        l_ref[:, cols] = l_ref[:, cols] * fade + jnp.sum(weights, 0, keepdims=True)
        attended = jnp.dot(
            kv_ref[score_rows:, 0:key_count],
            weights.astype(jnp.bfloat16),
            preferred_element_type=jnp.float32,
        )
        acc_ref[:, cols] = acc_ref[:, cols] * fade + attended
        m_ref[:, cols] = new_max

    @pl.when(block < own)
    def _():
        for tile in range(width // QTILE):
            visit(tile, width, False)

    @pl.when(block == own)
    def _():
        for tile in range(width // QTILE):
            visit(tile, (tile + 1) * QTILE, True)
        out_ref[...] = (acc_ref[...] / l_ref[...]).astype(out_ref.dtype)


def attention(own_index, queries, keyvals):
    rows, width = queries.shape
    kv_rows = rows + VDIM
    blocks = keyvals.shape[0] // kv_rows
    return pl.pallas_call(
        attention_kernel,
        out_shape=jax.ShapeDtypeStruct((VDIM, width), jnp.bfloat16),
        grid_spec=pltpu.PrefetchScalarGridSpec(
            num_scalar_prefetch=1,
            grid=(blocks,),
            in_specs=[
                pl.BlockSpec((rows, width), lambda i, own: (0, 0)),
                pl.BlockSpec((kv_rows, width), lambda i, own: (jnp.minimum(i, own[0]), 0)),
            ],
            out_specs=pl.BlockSpec((VDIM, width), lambda i, own: (0, 0)),
            scratch_shapes=[
                pltpu.VMEM((1, width), jnp.float32),
                pltpu.VMEM((1, width), jnp.float32),
                pltpu.VMEM((VDIM, width), jnp.float32),
            ],
        ),
        compiler_params=pltpu.CompilerParams(
            dimension_semantics=("arbitrary",), vmem_limit_bytes=40 << 20
        ),
        cost_estimate=pl.CostEstimate(
            flops=20_000_000_000, bytes_accessed=5_000_000, transcendentals=8_000_000
        ),
        name="attention",
    )(own_index.reshape(1).astype(jnp.int32), queries, keyvals)


def body(
    q_latent,
    kv_latent,
    rope_key,
    q_gain,
    kv_gain,
    w_query,
    w_keyval,
    w_output,
    moe_input,
    moe_gain,
    routes,
    route_weight,
    expert_gate,
    expert_up,
    expert_down,
    shared_gate,
    shared_up,
    shared_down,
):
    f32, bf16 = jnp.float32, jnp.bfloat16
    row_count = q_latent.shape[0]
    own_index = lax.axis_index("ep")
    ep_count = lax.axis_size("ep")
    tp_count = lax.axis_size("tp")
    width = moe_input.shape[1]
    top_count = routes.shape[1]

    own_block = lax.axis_index("tp")
    own_input = lax.dynamic_slice_in_dim(moe_input, own_block * MOE_DEV, MOE_DEV, 0)
    own_normed = layer_scale(own_input, moe_gain)
    own_routes = lax.dynamic_slice_in_dim(routes, own_block * MOE_DEV, MOE_DEV, 0)
    own_weight = lax.dynamic_slice_in_dim(route_weight, own_block * MOE_DEV, MOE_DEV, 0)
    experts = jnp.arange(ep_count, dtype=jnp.int32)
    named = (own_routes[:, :, None] == experts).astype(f32)
    in_row = jnp.sum(named, 1)
    token_at = jnp.arange(MOE_DEV)
    before = (token_at[None, :] < token_at[:, None]).astype(f32)
    rank = jnp.dot(before, in_row, preferred_element_type=f32)
    slot_at = jnp.arange(PAD, dtype=f32)
    taken = jnp.where(
        (in_row[:, :, None] > 0) & (rank[:, :, None] == slot_at), 1.0, 0.0
    )
    weight_of = jnp.sum(named * own_weight[:, :, None], 1)
    combine = (taken * weight_of[:, :, None]).reshape(MOE_DEV, ep_count * PAD)
    select = taken.reshape(MOE_DEV, ep_count * PAD).astype(bf16)
    outgoing = lax.dot_general(
        select, own_normed, (((0,), (0,)), ((), ())), preferred_element_type=f32
    ).astype(bf16)
    arrived = lax.all_to_all(outgoing, "ep", split_axis=0, concat_axis=0, tiled=True)
    squeeze = (
        jnp.arange(ep_count * PAD)[None, :]
        == (jnp.arange(ep_count * CAP) // CAP * PAD + jnp.arange(ep_count * CAP) % CAP)[:, None]
    ).astype(bf16)
    compact = jnp.dot(squeeze, arrived, preferred_element_type=f32).astype(bf16)
    inputs = lax.all_gather(compact, "tp", axis=0, tiled=True)

    positions = own_index * row_count + jnp.arange(row_count, dtype=jnp.int32)
    cosine_table, sine_table = rotary_tables(positions)
    q_normed = rms_scale(q_latent, q_gain)
    kv_normed = rms_scale(kv_latent, kv_gain)
    key_rotated = rotate_rows(rope_key.T.astype(f32), cosine_table, sine_table).astype(bf16)
    projected = lax.dot_general(
        w_query, q_normed, (((0,), (1,)), ((), ())), preferred_element_type=f32
    )
    queries = jnp.concatenate(
        [projected[:NOPE], rotate_rows(projected[NOPE:], cosine_table, sine_table)], 0
    ).astype(bf16)
    expanded = lax.dot_general(
        w_keyval, kv_normed, (((0,), (1,)), ((), ())), preferred_element_type=f32
    ).astype(bf16)
    own_keyvals = jnp.concatenate([expanded[:NOPE], key_rotated, expanded[NOPE:]], 0)
    keyvals = lax.all_gather(own_keyvals, "ep", axis=0, tiled=True)

    heads_own = attention(own_index, queries, keyvals)
    heads_out = lax.all_gather(heads_own, "tp", axis=0, tiled=True)
    mixed = lax.dot_general(
        heads_out, w_output, (((0,), (0,)), ((), ())), preferred_element_type=f32
    ).astype(bf16)

    normed = layer_scale(moe_input, moe_gain)
    shared_hidden = jax.nn.silu(jnp.dot(normed, shared_gate, preferred_element_type=f32))
    shared_hidden = (shared_hidden * jnp.dot(normed, shared_up, preferred_element_type=f32)).astype(
        bf16
    )
    shared_part = jnp.dot(shared_hidden, shared_down, preferred_element_type=f32).astype(bf16)

    hidden = jax.nn.silu(jnp.dot(inputs, expert_gate[0], preferred_element_type=f32))
    hidden = (hidden * jnp.dot(inputs, expert_up[0], preferred_element_type=f32)).astype(bf16)
    routed_part = jnp.dot(hidden, expert_down[0], preferred_element_type=f32).astype(bf16)
    routed_total = lax.psum_scatter(routed_part, "tp", scatter_dimension=0, tiled=True)
    shared_total = lax.psum_scatter(shared_part, "tp", scatter_dimension=0, tiled=True)
    spread = lax.dot_general(
        squeeze, routed_total, (((0,), (0,)), ((), ())), preferred_element_type=f32
    ).astype(bf16)
    returned = lax.all_to_all(spread, "ep", split_axis=0, concat_axis=0, tiled=True)
    combine_high = combine.astype(bf16)
    combine_low = (combine - combine_high.astype(f32)).astype(bf16)
    moe_out = (
        jnp.dot(combine_high, returned, preferred_element_type=f32)
        + jnp.dot(combine_low, returned, preferred_element_type=f32)
        + shared_total.astype(f32)
    ).astype(bf16)
    return (mixed, moe_out)


def solution(mesh):
    in_specs = (
        P("ep", None),
        P("ep", None),
        P("ep", None),
        P(),
        P(),
        P(None, "tp"),
        P(None, "tp"),
        P(None, "tp"),
        P("ep", None),
        P(),
        P("ep", None),
        P("ep", None),
        P("ep", None, "tp"),
        P("ep", None, "tp"),
        P("ep", "tp", None),
        P(None, "tp"),
        P(None, "tp"),
        P("tp", None),
    )
    out_specs = (P("ep", "tp"), P(("ep", "tp"), None))
    return jax.shard_map(body, mesh=mesh, in_specs=in_specs, out_specs=out_specs, check_vma=False)
```

time: 402 us -> 320 us (0.80)
  waiting for transfers between devices: 29.9 us -> 200 us
  local copies, waits for them, and re-layouts: 97.8 us -> 6.15 us
  blocking collectives: 84.7 us -> 0 us
  matrix products: 97.2 us -> 36.2 us
  Pallas kernels: 0 us -> 41 us
  other arithmetic: 29.5 us -> 5.58 us
  loops' own time: 20.9 us -> 0 us
  starting transfers between devices: 18.2 us -> 13.7 us
    all_gather x3, waiting for transfers between devices: 24 us -> 123 us  [the longest x1 46.6 us: body(): inputs = lax.all_gather(compact, 'tp', axis=0, tiled=True)]
    all_to_all x1 -> x0, blocking collectives: 84.7 us -> none  [body(): lax.all_to_all(outgoing, 'ep', split_axis=0, concat_axis=0, tiled=True)]
    reduce_scatter x2, waiting for transfers between devices: 0.05 us -> 68.8 us  [the longest x1 54.2 us: body(): lax.psum_scatter(shared_part, 'tp', scatter_dimension=0, tiled=True)]
    dot_general x62 -> x13, matrix products: 97.2 us -> 36.2 us  [the longest x1 12.6 us: body(): jnp.dot(hidden, expert_down[0], preferred_element_type=f32).astype(bf16)]
    pallas_call x0 -> x1, Pallas kernels: none -> 41 us  [attention(): pl.pallas_call(attention_kernel, out_shape=jax.ShapeDtypeStruct((VDIM, wi...]
    another operation x3 -> x0, local copies, waits for them, and re-layouts: 33.1 us -> none  [the longest x2 21.9 us: body(): partial_value = jnp.stack(results, 1)]
    another operation x17 -> x0, loops' own time: 20.9 us -> none  [the longest x1 11 us: body(): lax.scan(visit_block, carried, jnp.arange(block_count, dtype=jnp.int32))]
    gather x4 -> x0, local copies, waits for them, and re-layouts: 19.1 us -> none  [the longest x2 18 us: body(): normed[jnp.maximum(slot_token, 0)]]
  transfers between devices with their start and end apart: 6 -> 7, of which waited for: 2 -> 6; matrix products, arithmetic and copies ran while one was open for 55% -> 11% of each run, Pallas kernels for 0% -> 13%
where the time goes in v1:
time: 320 us; the launch traced here: 317 us
  waiting for transfers between devices  200 us (62%)
  Pallas kernels  41 us (13%)
  matrix products  36.2 us (11%)
  between operations  14.1 us (4%)
  starting transfers between devices  13.7 us (4%)
  local copies, waits for them, and re-layouts  6.15 us (2%)
  other arithmetic  5.58 us (2%)
    reduce_scatter x1, waiting for transfers between devices, body(): lax.psum_scatter(shared_part, 'tp', scatter_dimension=0, tiled=True)  54.2 us
    all_gather x1, waiting for transfers between devices, body(): inputs = lax.all_gather(compact, 'tp', axis=0, tiled=True)  46.6 us
    all_gather x1, waiting for transfers between devices, body(): keyvals = lax.all_gather(own_keyvals, 'ep', axis=0, tiled=True)  41.5 us
    pallas_call x1, Pallas kernels, attention(): pl.pallas_call(attention_kernel, out_shape=jax.ShapeDtypeStruct((VDIM, wi...  41 us
    all_gather x1, waiting for transfers between devices, body(): heads_out = lax.all_gather(heads_own, 'tp', axis=0, tiled=True)  35 us
    reduce_scatter x1, waiting for transfers between devices, body(): lax.psum_scatter(routed_part, 'tp', scatter_dimension=0, tiled=True)  14.6 us
    dot_general x1, matrix products, body(): jnp.dot(hidden, expert_down[0], preferred_element_type=f32).astype(bf16)  12.6 us
    all_to_all x1, waiting for transfers between devices, body(): lax.all_to_all(outgoing, 'ep', split_axis=0, concat_axis=0, tiled=True)  7.75 us
  transfers between devices with their start and end apart: 7, of which 6 were waited for; matrix products, arithmetic and copies ran while one was open for 11% of the time, Pallas kernels for 13%

profile of v1, /device:TPU:27, one launch (start us, length us, event | category | flops | bytes accessed | tf_op | source)
XLA Modules:
  0.0 316.6 jit_solution(12256373959500081566)
XLA Ops:
  7.2 0.9 constant_dynamic-slice_fusion
  8.1 0.7 constant_dynamic-slice_fusion.1
  8.9 0.1 fusion.85
  9.0 1.0 convert_reduce_fusion.1
  10.0 1.1 fusion.34
  11.2 0.1 eq.72
  11.3 2.1 fusion.6
  13.4 6.7 %all-to-all-start = ((bf16[16,8,2048]{2,1,0:T(8,128)(2,1)}), bf16[16,8,2048]{2,1,0:T(8,128)(2,1)S(1)}, u32[]{:S(2)}, u32[]{:S(2)}) async-start(bf16[16,8,2048]{2,1,0:T(8,128)(2,1)} %fusion.6), calls=%async_computation | async-start | bytes 1048576 | tf_op jit(solution)/shard_map/all_to_all | solution.py:190
  20.1 0.0 all-gather.8.cloned.1.call-start
  20.2 7.7 %all-to-all-done = bf16[16,8,2048]{2,1,0:T(8,128)(2,1)S(1)} async-done(((bf16[16,8,2048]{2,1,0:T(8,128)(2,1)}), bf16[16,8,2048]{2,1,0:T(8,128)(2,1)S(1)}, u32[]{:S(2)}, u32[]{:S(2)}) %all-to-all-start) | async-done | bytes 524320 | tf_op jit(solution)/shard_map/all_to_all | solution.py:190
  27.9 1.1 convolution_convert_fusion.4
  29.0 0.0 all-gather.8.cloned.1.call-update
  29.0 0.0 all-gather.4.cloned.1.call-start
  29.1 0.2 fusion.16
  29.3 0.3 fusion.11
  29.7 0.6 convolution_bitcast_fusion.2
  30.3 0.3 fusion.61
  30.6 0.4 fusion.14
  31.1 0.8 pad_maximum_fusion
  31.9 0.0 all-gather.4.cloned.1.call-update
  31.9 0.0 reduce-scatter.3.cloned.1.call-start
  31.9 46.6 %all-gather.8.cloned.1.call-done = bf16[1536,2048]{1,0:T(8,128)(2,1)} async-done(((bf16[96,2048]{1,0:T(8,128)(2,1)}), bf16[1536,2048]{1,0:T(8,128)(2,1)}) %all-gather.8.cloned.1.call-update) | async-done | bytes 6291472 | tf_op jit(solution)/shard_map/all_gather | solution.py:196
  78.6 6.0 %fusion.23 = f32[1536,256]{1,0:T(8,128)} fusion(bf16[1536,2048]{1,0:T(8,128)(2,1)} %all-gather.8.cloned.1.call-done, bf16[1,2048,256]{2,1,0:T(8,128)(2,1)} %param.30), kind=kOutput, calls=%fused_computation.39 | convolution fusion | flops 1610612736 | bytes 8912896 | tf_op jit(solution)/shard_map/dot_general | solution.py:228
  84.6 12.6 %convolution_convert_fusion = bf16[1536,2048]{1,0:T(8,128)(2,1)} fusion(bf16[1536,2048]{1,0:T(8,128)(2,1)} %all-gather.8.cloned.1.call-done, f32[1536,256]{1,0:T(8,128)} %fusion.23, bf16[1,256,2048]{2,1,0:T(8,128)(2,1)S(1)} %copy-done, bf16[1,2048,256]{2,1,0:T(8,128)(2,1)} %param.31), kind=kOutput, calls=%fused_computation | convolution fusion | flops 3226730496 | bytes 16252928 | tf_op jit(solution)/shard_map/dot_general | solution.py:230
  97.2 0.0 reduce-scatter.3.cloned.1.call-update
  97.2 0.2 all-gather.6.cloned.1.call-start
  97.5 41.5 %all-gather.4.cloned.1.call-done.kv_ref = bf16[2560,1024]{1,0:T(8,128)(2,1)} async-done(((bf16[160,1024]{1,0:T(8,128)(2,1)}), bf16[2560,1024]{1,0:T(8,128)(2,1)}) %all-gather.4.cloned.1.call-update) | async-done | bytes 5242896 | tf_op jit(solution)/shard_map/all_gather | solution.py:213
  139.0 2.5 copy-done.1
  141.5 41.0 %attention.1 = bf16[64,1024]{1,0:T(8,128)(2,1)} custom-call(s32[1]{0:T(128)} %bitcast.own_ref, bf16[96,1024]{1,0:T(8,128)(2,1)S(1)} %pad_maximum_fusion.1.q_ref, bf16[2560,1024]{1,0:T(8,128)(2,1)S(1)} %copy-done.1), custom_call_target="tpu_custom_call" | custom-call | flops 20000000000 | bytes 5000000 | tf_op jit(solution)/shard_map/attention/pallas_call | solution.py:114
  182.5 0.0 all-gather.6.cloned.1.call-update
  182.6 0.0 reduce-scatter.5.cloned.1.call-start
  182.6 0.3 convert_reduce_fusion
  183.0 0.7 fusion.2
  183.7 0.7 fusion.4
  184.4 1.3 copy-done.3
  185.7 0.7 fusion.98
  186.5 0.3 copy-done.7
  186.8 0.2 copy-done.8
  186.9 5.3 %convolution_convert_fusion.1 = bf16[512,2048]{1,0:T(8,128)(2,1)} fusion(bf16[128,2048]{1,0:T(8,128)(2,1)S(1)} %copy-done.7, bf16[512,2048]{1,0:T(8,128)(2,1)} %copy-done.3, bf16[2048,128]{1,0:T(8,128)(2,1)S(1)} %copy-done.8, f32[512,128]{1,0:T(8,128)S(1)} %fusion.98), kind=kOutput, calls=%fused_computation.8 | convolution fusion | flops 538312704 | bytes 5505024 | tf_op jit(solution)/shard_map/dot_general | solution.py:226
  192.2 0.0 reduce-scatter.5.cloned.1.call-update
  192.2 14.6 %reduce-scatter.3.cloned.1.call-done = bf16[96,2048]{1,0:T(8,128)(2,1)} async-done(((bf16[1536,2048]{1,0:T(8,128)(2,1)}), bf16[96,2048]{1,0:T(8,128)(2,1)}) %reduce-scatter.3.cloned.1.call-update) | async-done | bytes 393232 | tf_op jit(solution)/shard_map/reduce_scatter | solution.py:231
  206.9 2.2 fusion.7
  209.1 6.6 %all-to-all-start.1 = ((bf16[16,8,2048]{2,1,0:T(8,128)(2,1)}), bf16[16,8,2048]{2,1,0:T(8,128)(2,1)S(1)}, u32[]{:S(2)}, u32[]{:S(2)}) async-start(bf16[16,8,2048]{2,1,0:T(8,128)(2,1)} %fusion.7), calls=%async_computation.2 | async-start | bytes 1048576 | tf_op jit(solution)/shard_map/all_to_all | solution.py:236
  215.7 35.0 %all-gather.6.cloned.1.call-done = bf16[1024,1024]{1,0:T(8,128)(2,1)} async-done(((bf16[64,1024]{1,0:T(8,128)(2,1)}), bf16[1024,1024]{1,0:T(8,128)(2,1)}) %all-gather.6.cloned.1.call-update) | async-done | bytes 2097168 | tf_op jit(solution)/shard_map/all_gather | solution.py:216
  250.7 3.1 convolution_convert_fusion.5
  253.7 0.3 convolution_bitcast_fusion
  254.0 54.2 %reduce-scatter.5.cloned.1.call-done = bf16[32,2048]{1,0:T(8,128)(2,1)} async-done(((bf16[512,2048]{1,0:T(8,128)(2,1)}), bf16[32,2048]{1,0:T(8,128)(2,1)}) %reduce-scatter.5.cloned.1.call-update) | async-done | bytes 131088 | tf_op jit(solution)/shard_map/reduce_scatter | solution.py:232
  308.2 1.8 fusion.10
  (45 shorter events, 0.2 us)
Async XLA Ops:
  7.2 77.4 %copy-start = (bf16[1,256,2048]{2,1,0:T(8,128)(2,1)S(1)}, bf16[1,256,2048]{2,1,0:T(8,128)(2,1)}, u32[]{:S(2)}) copy-start(bf16[1,256,2048]{2,1,0:T(8,128)(2,1)} %param.32) | copy-start | bytes 3145732
  7.2 21.9 %copy-start.5 = (bf16[1024,256]{1,0:T(8,128)(2,1)S(1)}, bf16[1024,256]{1,0:T(8,128)(2,1)}, u32[]{:S(2)}) copy-start(bf16[1024,256]{1,0:T(8,128)(2,1)} %param.19) | copy-start | bytes 1572868
  7.2 22.1 %copy-start.4 = (bf16[1024,512]{1,0:T(8,128)(2,1)S(1)}, bf16[1024,512]{1,0:T(8,128)(2,1)}, u32[]{:S(2)}) copy-start(bf16[1024,512]{1,0:T(8,128)(2,1)} %param.18) | copy-start | bytes 3145732
  13.4 16.3 %copy-start.10 = (bf16[1024,32]{0,1:T(8,128)(2,1)S(1)}, bf16[1024,32]{0,1:T(8,128)(2,1)}, u32[]{:S(2)}) copy-start(bf16[1024,32]{0,1:T(8,128)(2,1)} %param.20) | copy-start | bytes 196612
  13.4 16.3 %copy-start.12 = (bf16[512,96]{0,1:T(8,128)(2,1)S(1)}, bf16[512,96]{0,1:T(8,128)(2,1)}, u32[]{:S(2)}) copy-start(bf16[512,96]{0,1:T(8,128)(2,1)} %param.23) | copy-start | bytes 294916
  13.4 16.3 %copy-start.14 = (f32[512]{0:T(512)S(1)}, f32[512]{0:T(512)}, u32[]{:S(2)}) copy-start(f32[512]{0:T(512)} %param.21) | copy-start | bytes 6148
  13.4 14.5 %all-to-all-start = ((bf16[16,8,2048]{2,1,0:T(8,128)(2,1)}), bf16[16,8,2048]{2,1,0:T(8,128)(2,1)S(1)}, u32[]{:S(2)}, u32[]{:S(2)}) async-start(bf16[16,8,2048]{2,1,0:T(8,128)(2,1)} %fusion.6), calls=%async_computation | async-start | bytes 1048576 | tf_op jit(solution)/shard_map/all_to_all | solution.py:190
  20.1 58.5 %all-gather.8.cloned.1.call-start = ((), (), s32[]{:S(2)}) async-start(), calls=%async_computation.6 | async-start | bytes 6684672 | tf_op jit(solution)/shard_map/all_gather | solution.py:196
  29.0 110.0 %all-gather.4.cloned.1.call-start = ((), (), s32[]{:S(2)}) async-start(), calls=%async_computation.4 | async-start | bytes 5570560 | tf_op jit(solution)/shard_map/all_gather | solution.py:213
  29.1 1.5 copy-start.13
  29.1 1.5 copy-start.15
  31.9 175.0 %reduce-scatter.3.cloned.1.call-start = ((), (), s32[]{:S(2)}) async-start(), calls=%async_computation.7 | async-start | bytes 6684672 | tf_op jit(solution)/shard_map/reduce_scatter | solution.py:231
  97.2 153.4 %all-gather.6.cloned.1.call-start = ((), (), s32[]{:S(2)}) async-start(), calls=%async_computation.5 | async-start | bytes 2228224 | tf_op jit(solution)/shard_map/all_gather | solution.py:216
  139.0 2.5 copy-start.1
  141.5 41.1 %copy-start.2 = (bf16[512,2048]{1,0:T(8,128)(2,1)S(1)}, bf16[512,2048]{1,0:T(8,128)(2,1)}, u32[]{:S(2)}) copy-start(bf16[512,2048]{1,0:T(8,128)(2,1)} %param.26) | copy-start | bytes 6291460
  182.6 1.1 copy-start.11
  182.6 125.6 %reduce-scatter.5.cloned.1.call-start = ((), (), s32[]{:S(2)}) async-start(), calls=%async_computation.8 | async-start | bytes 2228224 | tf_op jit(solution)/shard_map/reduce_scatter | solution.py:232
  183.7 2.0 copy-start.6
  184.4 1.3 copy-start.3
  185.7 1.1 copy-start.7
  185.7 1.2 copy-start.8
  192.2 58.5 %copy-start.9 = (bf16[1024,128]{1,0:T(8,128)(2,1)S(1)}, bf16[1024,128]{1,0:T(8,128)(2,1)}, u32[]{:S(2)}) copy-start(bf16[1024,128]{1,0:T(8,128)(2,1)} %param.25) | copy-start | bytes 786436
  209.1 44.7 %all-to-all-start.1 = ((bf16[16,8,2048]{2,1,0:T(8,128)(2,1)}), bf16[16,8,2048]{2,1,0:T(8,128)(2,1)S(1)}, u32[]{:S(2)}, u32[]{:S(2)}) async-start(bf16[16,8,2048]{2,1,0:T(8,128)(2,1)} %fusion.7), calls=%async_computation.2 | async-start | bytes 1048576 | tf_op jit(solution)/shard_map/all_to_all | solution.py:236
Sparse Core Ops, SparseCore 0:
  29.1 49.4 all-gather.7
  81.0 57.9 all-gather.3
  141.6 65.2 reduce-scatter.2
  209.1 41.5 all-gather.5
  253.0 55.1 reduce-scatter.4

commit v2 on v1

v2 whole, which is shorter than its diff:
```python
import functools

import jax
import jax.numpy as jnp
from jax import lax
from jax.experimental import pallas as pl
from jax.experimental.pallas import tpu as pltpu
from jax.sharding import PartitionSpec as P

NOPE = 64
ROPE_DIM = 32
VDIM = 64
MOE_DEV = 32
CAP = 6
PAD = 8

norm_eps = 1e-06
layer_eps = 1e-05
rotary_base = 10000.0
floor_value = -1e30
QTILE = 256
LOG2E = 1.4426950408889634


def rms_scale(values, gain):
    widened = values.astype(jnp.float32)
    return (
        widened * lax.rsqrt(jnp.mean(widened * widened, -1, keepdims=True) + norm_eps) * gain
    ).astype(jnp.bfloat16)


def layer_scale(values, gain):
    widened = values.astype(jnp.float32)
    centred = widened - jnp.mean(widened, -1, keepdims=True)
    return (
        centred * lax.rsqrt(jnp.mean(centred * centred, -1, keepdims=True) + layer_eps) * gain
    ).astype(jnp.bfloat16)


def rotary_tables(positions):
    halfway = ROPE_DIM // 2
    inverse = rotary_base ** (-(jnp.arange(halfway, dtype=jnp.float32) * 2.0 / ROPE_DIM))
    angles = positions.astype(jnp.float32)[None, :] * inverse[:, None]
    return (jnp.cos(angles), jnp.sin(angles))


def rotate_rows(values, cosine_table, sine_table):
    halfway = values.shape[0] // 2
    first_half = values[:halfway]
    second_half = values[halfway:]
    return jnp.concatenate(
        [
            first_half * cosine_table - second_half * sine_table,
            second_half * cosine_table + first_half * sine_table,
        ],
        0,
    )


MESH = pl.DeviceIdType.MESH


def fused_kernel(
    ep_count,
    z_count,
    outgoing_ref,
    q_ref,
    own_kv_ref,
    normed_ref,
    gate_ref,
    up_ref,
    down_ref,
    sgate_ref,
    sup_ref,
    sdown_ref,
    chigh_ref,
    clow_ref,
    wout_ref,
    mixed_ref,
    moe_ref,
    recv_a,
    buf_x,
    buf_p,
    recv_d,
    buf_s,
    recv_r,
    final,
    kv,
    heads,
    send_b,
    recv_b,
    q_t,
    m_t,
    l_t,
    acc_t,
    a_send,
    a_recv,
    k_send,
    k_recv,
    x_send,
    x_recv,
    xd_send,
    xd_recv,
    p_send,
    p_recv,
    r_send,
    r_recv,
    h_send,
    h_recv,
    hd_send,
    hd_recv,
    b_send,
    b_recv,
):
    f32, bf16 = jnp.float32, jnp.bfloat16
    ep = lax.axis_index("ep")
    tp = lax.axis_index("tp")
    z = lax.div(tp, 2)
    core = lax.rem(tp, 2)
    other = 1 - core
    half_ring = z_count // 2
    steps = half_ring - 1
    slots = ep_count * CAP
    rows = slots + MOE_DEV
    width = normed_ref.shape[1]
    score_rows = NOPE + ROPE_DIM
    length = q_ref.shape[1]
    tiles = length // QTILE
    scale = float(score_rows) ** (-0.5) * LOG2E
    partner = {"tp": z * 2 + other}
    x_half = slots // 2
    r_half = rows // 2
    r_cols = width // 2
    h_half = VDIM // 2

    def around(offset):
        return lax.rem(z + offset + 2 * z_count, z_count)

    def at_z(offset):
        return {"tp": around(offset) * 2 + core}

    def at_ep(offset):
        return {"ep": lax.rem(ep + offset + ep_count, ep_count)}

    def remote(src, dst, send, recv, device):
        return pltpu.make_async_remote_copy(
            src_ref=src, dst_ref=dst, send_sem=send, recv_sem=recv,
            device_id=device, device_id_type=MESH,
        )

    def loop(low, high, step):
        def run(index, carry):
            step(index)
            return carry

        lax.fori_loop(low, high, run, 0)

    barrier = pltpu.get_barrier_semaphore()
    loop(1, ep_count, lambda d: pl.semaphore_signal(
        barrier, inc=1, device_id=at_ep(d), device_id_type=MESH))
    for device in (at_z(1), at_z(-1), partner):
        pl.semaphore_signal(barrier, inc=1, device_id=device, device_id_type=MESH)
    pl.semaphore_wait(barrier, ep_count + 2)

    def a_copy(d):
        there = lax.rem(ep + d, ep_count)
        return remote(outgoing_ref.at[there], recv_a.at[ep], a_send.at[d], a_recv.at[d], at_ep(d))

    def a_arrival(d):
        source = lax.rem(ep - d + ep_count, ep_count)
        return remote(outgoing_ref.at[ep], recv_a.at[source], a_send.at[d], a_recv.at[d], at_ep(d))

    def k_copy(d):
        return remote(own_kv_ref, kv.at[ep], k_send.at[d], k_recv.at[d], at_ep(d))

    def k_arrival(d):
        source = lax.rem(ep - d + ep_count, ep_count)
        return remote(own_kv_ref, kv.at[source], k_send.at[d], k_recv.at[d], at_ep(d))

    def guarded(test, act):
        @pl.when(test)
        def _():
            act()

    loop(1, ep_count, lambda d: a_copy(d).start())
    loop(1, ep_count, lambda d: guarded(ep + d < ep_count, lambda: k_copy(d).start()))
    recv_a[ep] = outgoing_ref[ep]

    def shared_rows(first, count):
        x = normed_ref[pl.ds(first * count * 2 * MOE_DEV, count * 2 * MOE_DEV), :]
        hidden = jax.nn.silu(jnp.dot(x, sgate_ref[...], preferred_element_type=f32))
        hidden = (hidden * jnp.dot(x, sup_ref[...], preferred_element_type=f32)).astype(bf16)
        part = jnp.dot(hidden, sdown_ref[...], preferred_element_type=f32).astype(bf16)
        for at in range(count):
            for side in range(2):
                begin = (at * 2 + side) * MOE_DEV
                buf_p[first * count + at, side, slots:rows, :] = part[begin : begin + MOE_DEV]

    per_call = 2
    loop(0, z_count // per_call, lambda first: shared_rows(first, per_call))

    for tile in range(tiles):
        q_t[tile] = q_ref[:, tile * QTILE : (tile + 1) * QTILE]
    m_t[...] = jnp.full_like(m_t, floor_value)
    l_t[...] = jnp.zeros_like(l_t)
    acc_t[...] = jnp.zeros_like(acc_t)

    def squeeze_rows(shape, slot_dim):
        slot = lax.broadcasted_iota(jnp.int32, shape, slot_dim)
        place = lax.broadcasted_iota(jnp.int32, shape, 1 - slot_dim)
        return jnp.where(
            place == lax.div(slot, CAP) * PAD + lax.rem(slot, CAP), 1.0, 0.0
        ).astype(bf16)

    loop(1, ep_count, lambda d: a_arrival(d).wait_recv())
    arrived = recv_a[...].astype(f32).reshape(ep_count * PAD, width).astype(bf16)
    buf_x[z, core] = jnp.dot(
        squeeze_rows((slots, ep_count * PAD), 0), arrived, preferred_element_type=f32
    ).astype(bf16)

    def ring_copy(buf, send, recv, size, side, step, half, origin):
        part = pl.ds(half * size, size)
        return remote(
            buf.at[origin, core, part], buf.at[origin, core, part],
            send.at[side, step, half], recv.at[side, step, half], at_z(1 - 2 * side),
        )

    def hand_copy(buf, send, recv, size, offset, half, whose):
        part = pl.ds(half * size, size)
        here = buf.at[around(offset), whose, part]
        return remote(here, here, send.at[offset, half], recv.at[offset, half], partner)

    def x_ring(side, step, half, origin):
        return ring_copy(buf_x, x_send, x_recv, x_half, side, step, half, origin)

    def x_hand(offset, half, whose):
        return hand_copy(buf_x, xd_send, xd_recv, x_half, offset, half, whose)

    def h_ring(side, step, half, origin):
        return ring_copy(heads, h_send, h_recv, h_half, side, step, half, origin)

    def h_hand(offset, half, whose):
        return hand_copy(heads, hd_send, hd_recv, h_half, offset, half, whose)

    def offset_of(side, step):
        return step if side else z_count - step

    def begin_gather(ring, hand):
        for half in range(2):
            for side in range(2):
                ring(side, 1, half, z).start()
            hand(0, half, core).start()

    def pass_on(ring, hand, step):
        for half in range(2):
            for side in range(2):
                offset = offset_of(side, step)
                origin = around(offset)
                ring(side, step, half, origin).wait_recv()
                if half == side:
                    ring(side, step + 1, half, origin).start()
                else:
                    guarded(step < steps, lambda: ring(side, step + 1, half, origin).start())
                hand(offset, half, core).start()

    def pass_last(ring, hand):
        origin = around(half_ring)
        for side in range(2):
            ring(side, half_ring, side, origin).wait_recv()
            hand(half_ring, side, core).start()

    def take_hand(hand, offset):
        for half in range(2):
            hand(offset, half, other).wait_recv()

    def p_copy(offset):
        at = around(offset)
        return remote(buf_p.at[at, other], recv_d.at[at], p_send.at[offset], p_recv.at[offset], partner)

    def expert(offset):
        at = around(offset)
        x = buf_x[at].reshape(2 * slots, width)
        hidden = jax.nn.silu(jnp.dot(x, gate_ref[...], preferred_element_type=f32))
        hidden = (hidden * jnp.dot(x, up_ref[...], preferred_element_type=f32)).astype(bf16)
        part = jnp.dot(hidden, down_ref[...], preferred_element_type=f32).astype(bf16)
        for side in range(2):
            buf_p[at, side, 0:slots, :] = part[side * slots : (side + 1) * slots]
        p_copy(offset).start()

    def pair_sum(offset):
        at = around(offset)
        p_copy(offset).wait_recv()
        for half in range(2):
            for side in range(2):
                part = (slice(half * r_half, (half + 1) * r_half), slice(side * r_cols, (side + 1) * r_cols))
                buf_s[at, side, half] = (
                    buf_p[(at, core) + part].astype(f32) + recv_d[(at,) + part].astype(f32)
                ).astype(bf16)

    def visit(block, tile, key_count, masked):
        scores = lax.dot_general(
            block[0:score_rows, 0:key_count],
            q_t[tile],
            (((0,), (0,)), ((), ())),
            preferred_element_type=f32,
        )
        if masked:
            key_at = lax.broadcasted_iota(jnp.int32, scores.shape, 0)
            query_at = tile * QTILE + lax.broadcasted_iota(jnp.int32, scores.shape, 1)
            scores = jnp.where(key_at <= query_at, scores, floor_value)
        old_max = m_t[tile]
        new_max = jnp.maximum(old_max, jnp.max(scores, 0, keepdims=True))
        weights = jnp.exp2((scores - new_max) * scale)
        fade = jnp.exp2((old_max - new_max) * scale)
        l_t[tile] = l_t[tile] * fade + jnp.sum(weights, 0, keepdims=True)
        attended = jnp.dot(
            block[score_rows:, 0:key_count], weights.astype(bf16), preferred_element_type=f32
        )
        acc_t[tile] = acc_t[tile] * fade + attended
        m_t[tile] = new_max

    def earlier_block(d):
        def act():
            k_arrival(d).wait_recv()
            for tile in range(tiles):
                visit(kv.at[ep - d], tile, length, False)

        guarded(d <= ep, act)

    early = 2 * steps

    def part_block(unit):
        d = early + 1 + lax.div(unit, 2)
        which = lax.rem(unit, 2)
        guarded(which == 0, lambda: k_arrival(d).wait_recv())
        for tile in range(tiles // 2):
            visit(kv.at[ep - d], which * (tiles // 2) + tile, length, False)

    begin_gather(x_ring, x_hand)
    for tile in range(tiles):
        visit(own_kv_ref, tile, (tile + 1) * QTILE, True)
    take_hand(x_hand, 0)
    expert(0)

    def gather_step(step):
        pass_on(x_ring, x_hand, step)
        for side in range(2):
            take_hand(x_hand, offset_of(side, step))
        loop(0, 2, lambda side: expert(lax.rem(step * (2 * side - 1) + z_count, z_count)))
        loop(2 * step - 1, 2 * step + 1, earlier_block)
        loop(0, 2, lambda side: pair_sum(lax.rem(step * (2 * side - 1) + z_count, z_count)))

    loop(1, half_ring, gather_step)
    pass_last(x_ring, x_hand)

    def r_copy(step, side, half, chunk):
        return remote(
            buf_s.at[chunk, side, half], recv_r.at[step, side, half],
            r_send.at[step, side, half], r_recv.at[step, side, half], at_z(1 - 2 * side),
        )

    for half in range(2):
        for side in range(2):
            r_copy(0, side, half, around(2 * side - 1)).start()
    pair_sum(0)
    take_hand(x_hand, half_ring)
    expert(half_ring)
    pair_sum(half_ring)

    events = 4 * (z_count - 2)
    units = 2 * jnp.maximum(ep - early, 0)

    def sum_event(event):
        step = lax.div(event, 4) + 1
        side = lax.rem(event, 2)
        half = lax.div(lax.rem(event, 4), 2)
        chunk = around((step + 1) * (2 * side - 1))
        r_copy(step - 1, side, half, chunk).wait_recv()
        buf_s[chunk, side, half] = (
            buf_s[chunk, side, half].astype(f32) + recv_r[step - 1, side, half].astype(f32)
        ).astype(bf16)
        r_copy(step, side, half, chunk).start()
        loop(lax.div(event * units, events), lax.div((event + 1) * units, events), part_block)

    loop(0, events, sum_event)

    for tile in range(tiles):
        heads[z, core, :, tile * QTILE : (tile + 1) * QTILE] = (acc_t[tile] / l_t[tile]).astype(bf16)
    begin_gather(h_ring, h_hand)

    for half in range(2):
        for side in range(2):
            r_copy(z_count - 2, side, half, z).wait_recv()
            final[half * r_half : (half + 1) * r_half, side * r_cols : (side + 1) * r_cols] = (
                buf_s[z, side, half].astype(f32) + recv_r[z_count - 2, side, half].astype(f32)
            )

    spread = jnp.dot(
        squeeze_rows((ep_count * PAD, slots), 1),
        final[0:slots, :].astype(bf16),
        preferred_element_type=f32,
    )
    send_b[...] = spread.reshape(ep_count, PAD, width).astype(bf16)

    def b_copy(d):
        there = lax.rem(ep + d, ep_count)
        return remote(send_b.at[there], recv_b.at[ep], b_send.at[d], b_recv.at[d], at_ep(d))

    def b_arrival(d):
        source = lax.rem(ep - d + ep_count, ep_count)
        return remote(send_b.at[ep], recv_b.at[source], b_send.at[d], b_recv.at[d], at_ep(d))

    loop(1, ep_count, lambda d: b_copy(d).start())
    recv_b[ep] = send_b[ep]

    loop(1, half_ring, lambda step: pass_on(h_ring, h_hand, step))
    pass_last(h_ring, h_hand)

    loop(1, ep_count, lambda d: b_arrival(d).wait_recv())
    returned = recv_b[...].astype(f32).reshape(ep_count * PAD, width).astype(bf16)
    moe_ref[...] = (
        jnp.dot(chigh_ref[...], returned, preferred_element_type=f32)
        + jnp.dot(clow_ref[...], returned, preferred_element_type=f32)
        + final[slots:rows, :]
    ).astype(bf16)

    loop(0, z_count, lambda offset: take_hand(h_hand, offset))
    mixed_ref[...] = lax.dot_general(
        heads[...].reshape(2 * z_count * VDIM, length),
        wout_ref[...],
        (((0,), (0,)), ((), ())),
        preferred_element_type=f32,
    ).astype(bf16)

    loop(1, ep_count, lambda d: a_copy(d).wait_send())
    loop(1, ep_count, lambda d: b_copy(d).wait_send())
    loop(1, ep_count, lambda d: guarded(ep + d < ep_count, lambda: k_copy(d).wait_send()))

    def left(step):
        for half in range(2):
            for side in range(2):
                x_ring(side, step, half, z).wait_send()
                h_ring(side, step, half, z).wait_send()

    loop(1, half_ring, left)
    for side in range(2):
        x_ring(side, half_ring, side, z).wait_send()
        h_ring(side, half_ring, side, z).wait_send()

    def handed(offset):
        for half in range(2):
            x_hand(offset, half, core).wait_send()
            h_hand(offset, half, core).wait_send()
        p_copy(offset).wait_send()

    loop(0, z_count, handed)

    def summed(step):
        for half in range(2):
            for side in range(2):
                r_copy(step, side, half, z).wait_send()

    loop(0, z_count - 1, summed)


def fused(ep_count, tp_count, width, operands):
    f32, bf16 = jnp.float32, jnp.bfloat16
    z_count = tp_count // 2
    half_ring = z_count // 2
    slots = ep_count * CAP
    rows = slots + MOE_DEV
    score_rows, length = operands[1].shape
    tiles = length // QTILE
    dma = pltpu.SemaphoreType.DMA
    vmem = pltpu.VMEM
    return pl.pallas_call(
        functools.partial(fused_kernel, ep_count, z_count),
        out_shape=(
            jax.ShapeDtypeStruct((length, operands[-1].shape[1]), bf16),
            jax.ShapeDtypeStruct((MOE_DEV, width), bf16),
        ),
        in_specs=[pl.BlockSpec(memory_space=pltpu.VMEM)] * len(operands),
        out_specs=(pl.BlockSpec(memory_space=pltpu.VMEM),) * 2,
        scratch_shapes=[
            vmem((ep_count, PAD, width), bf16),
            vmem((z_count, 2, slots, width), bf16),
            vmem((z_count, 2, rows, width), bf16),
            vmem((z_count, rows, width), bf16),
            vmem((z_count, 2, 2, rows // 2, width // 2), bf16),
            vmem((z_count - 1, 2, 2, rows // 2, width // 2), bf16),
            vmem((rows, width), f32),
            vmem((ep_count, score_rows + VDIM, length), bf16),
            vmem((z_count, 2, VDIM, length), bf16),
            vmem((ep_count, PAD, width), bf16),
            vmem((ep_count, PAD, width), bf16),
            vmem((tiles, score_rows, QTILE), bf16),
            vmem((tiles, 1, QTILE), f32),
            vmem((tiles, 1, QTILE), f32),
            vmem((tiles, VDIM, QTILE), f32),
            dma((ep_count,)),
            dma((ep_count,)),
            dma((ep_count,)),
            dma((ep_count,)),
            dma((2, half_ring + 1, 2)),
            dma((2, half_ring + 1, 2)),
            dma((z_count, 2)),
            dma((z_count, 2)),
            dma((z_count,)),
            dma((z_count,)),
            dma((z_count - 1, 2, 2)),
            dma((z_count - 1, 2, 2)),
            dma((2, half_ring + 1, 2)),
            dma((2, half_ring + 1, 2)),
            dma((z_count, 2)),
            dma((z_count, 2)),
            dma((ep_count,)),
            dma((ep_count,)),
        ],
        compiler_params=pltpu.CompilerParams(
            collective_id=0, has_side_effects=True, vmem_limit_bytes=62 << 20
        ),
        name="fused",
    )(*operands)


def body(
    q_latent,
    kv_latent,
    rope_key,
    q_gain,
    kv_gain,
    w_query,
    w_keyval,
    w_output,
    moe_input,
    moe_gain,
    routes,
    route_weight,
    expert_gate,
    expert_up,
    expert_down,
    shared_gate,
    shared_up,
    shared_down,
):
    f32, bf16 = jnp.float32, jnp.bfloat16
    row_count = q_latent.shape[0]
    own_index = lax.axis_index("ep")
    ep_count = lax.axis_size("ep")
    tp_count = lax.axis_size("tp")
    width = moe_input.shape[1]
    top_count = routes.shape[1]

    own_block = lax.axis_index("tp")
    own_input = lax.dynamic_slice_in_dim(moe_input, own_block * MOE_DEV, MOE_DEV, 0)
    own_normed = layer_scale(own_input, moe_gain)
    own_routes = lax.dynamic_slice_in_dim(routes, own_block * MOE_DEV, MOE_DEV, 0)
    own_weight = lax.dynamic_slice_in_dim(route_weight, own_block * MOE_DEV, MOE_DEV, 0)
    experts = jnp.arange(ep_count, dtype=jnp.int32)
    named = (own_routes[:, :, None] == experts).astype(f32)
    in_row = jnp.sum(named, 1)
    token_at = jnp.arange(MOE_DEV)
    before = (token_at[None, :] < token_at[:, None]).astype(f32)
    rank = jnp.dot(before, in_row, preferred_element_type=f32)
    slot_at = jnp.arange(PAD, dtype=f32)
    taken = jnp.where(
        (in_row[:, :, None] > 0) & (rank[:, :, None] == slot_at), 1.0, 0.0
    )
    weight_of = jnp.sum(named * own_weight[:, :, None], 1)
    combine = (taken * weight_of[:, :, None]).reshape(MOE_DEV, ep_count * PAD)
    select = taken.reshape(MOE_DEV, ep_count * PAD).astype(bf16)
    outgoing = (
        lax.dot_general(select, own_normed, (((0,), (0,)), ((), ())), preferred_element_type=f32)
        .astype(bf16)
        .reshape(ep_count, PAD, width)
    )
    positions = own_index * row_count + jnp.arange(row_count, dtype=jnp.int32)
    cosine_table, sine_table = rotary_tables(positions)
    q_normed = rms_scale(q_latent, q_gain)
    kv_normed = rms_scale(kv_latent, kv_gain)
    key_rotated = rotate_rows(rope_key.T.astype(f32), cosine_table, sine_table).astype(bf16)
    projected = lax.dot_general(
        w_query, q_normed, (((0,), (1,)), ((), ())), preferred_element_type=f32
    )
    queries = jnp.concatenate(
        [projected[:NOPE], rotate_rows(projected[NOPE:], cosine_table, sine_table)], 0
    ).astype(bf16)
    expanded = lax.dot_general(
        w_keyval, kv_normed, (((0,), (1,)), ((), ())), preferred_element_type=f32
    ).astype(bf16)
    own_keyvals = jnp.concatenate([expanded[:NOPE], key_rotated, expanded[NOPE:]], 0)
    normed = layer_scale(moe_input, moe_gain)
    combine_high = combine.astype(bf16)
    combine_low = (combine - combine_high.astype(f32)).astype(bf16)
    mixed, moe_out = fused(
        ep_count,
        tp_count,
        width,
        (
            outgoing,
            queries,
            own_keyvals,
            normed,
            expert_gate[0],
            expert_up[0],
            expert_down[0],
            shared_gate,
            shared_up,
            shared_down,
            combine_high,
            combine_low,
            w_output,
        ),
    )
    return (mixed, moe_out)


def solution(mesh):
    in_specs = (
        P("ep", None),
        P("ep", None),
        P("ep", None),
        P(),
        P(),
        P(None, "tp"),
        P(None, "tp"),
        P(None, "tp"),
        P("ep", None),
        P(),
        P("ep", None),
        P("ep", None),
        P("ep", None, "tp"),
        P("ep", None, "tp"),
        P("ep", "tp", None),
        P(None, "tp"),
        P(None, "tp"),
        P("tp", None),
    )
    out_specs = (P("ep", "tp"), P(("ep", "tp"), None))
    return jax.shard_map(body, mesh=mesh, in_specs=in_specs, out_specs=out_specs, check_vma=False)
```

time: 320 us -> 174 us (0.54)
  the two profiles are of different devices: /device:TPU:27 before, /device:TPU:19 now
where the time goes in v2:
time: 174 us
  Pallas kernels  154 us (89%)
  other arithmetic  10.6 us (6%)
  local copies, waits for them, and re-layouts  5.16 us (3%)
  matrix products  3.31 us (2%)
    pallas_call x1, Pallas kernels, fused(): pl.pallas_call(functools.partial(fused_kernel, ep_count, z_count), out_sh...  154 us

profile of v2, /device:TPU:19, one launch (start us, length us, event | category | flops | bytes accessed | tf_op | source)
XLA Modules:
  0.0 173.9 jit_solution(4300855130486660177)
XLA Ops:
  0.6 0.0 copy-start
  0.6 0.0 copy-start.1
  0.7 1.2 convert_reduce_fusion.1
  1.9 1.1 fusion.21
  3.0 0.8 constant_dynamic-slice_fusion.1
  3.8 0.7 constant_dynamic-slice_fusion
  4.5 0.0 copy-start.2
  4.5 2.0 %convert_reduce_fusion = f32[512]{0:T(512)S(1)} fusion(bf16[512,2048]{1,0:T(8,128)(2,1)} %param.26), kind=kLoop, calls=%fused_computation.1 | loop fusion | flops 2096640 | bytes 2099200 | tf_op jit(solution)/shard_map/reduce_sum | solution.py:34
  6.5 0.0 copy-start.3
  6.6 0.0 copy-done.1
  6.6 0.0 copy-start.4
  6.6 0.0 copy-start.6
  6.6 0.0 copy-start.8
  6.6 0.7 fusion.2
  7.3 0.0 copy-start.7
  7.3 0.0 copy-done.2
  7.3 0.3 fusion.6
  7.6 0.0 copy-done.3
  7.6 0.2 fusion.10
  7.9 0.1 eq.40
  8.0 0.1 fusion.45
  8.1 0.1 copy.29
  8.2 0.1 copy.28
  8.3 0.1 copy.30
  8.4 0.6 subtract_convert_fusion
  9.0 0.6 fusion.46.chigh_ref
  9.6 0.0 copy-done.4
  9.6 0.0 copy-done.6
  9.6 0.0 copy-done.8
  9.6 1.5 fusion.9
  11.1 0.0 copy-start.5
  11.2 0.0 copy-done
  11.2 0.0 copy-done.7
  11.2 0.6 convolution_bitcast_fusion
  11.8 0.3 fusion.42
  12.1 0.7 pad_maximum_fusion.own_kv_ref
  12.9 0.7 pad_maximum_fusion.1.q_ref
  13.6 0.0 copy-done.5
  13.6 1.1 fusion.5.outgoing_ref
  14.7 2.0 %fusion.4.normed_ref = bf16[512,2048]{1,0:T(8,128)(2,1)} fusion(bf16[512,2048]{1,0:T(8,128)(2,1)S(1)} %copy-done.1, f32[2048]{0:T(1024)S(1)} %copy-done.5, f32[512]{0:T(512)S(1)} %add_rsqrt_fusion.2, f32[512]{0:T(512)S(1)} %broadcast_multiply_fusion), kind=kLoop, calls=%fused_computation.6 | loop fusion | flops 5242880 | bytes 4206592 | tf_op jit(solution)/shard_map/convert_element_type | solution.py:37
  16.7 153.9 %fused.1 = (bf16[1024,128]{1,0:T(8,128)(2,1)}, bf16[32,2048]{1,0:T(8,128)(2,1)}) custom-call(bf16[16,8,2048]{2,1,0:T(8,128)(2,1)} %fusion.5.outgoing_ref, bf16[96,1024]{1,0:T(8,128)(2,1)} %pad_maximum_fusion.1.q_ref, bf16[160,1024]{1,0:T(8,128)(2,1)} %pad_maximum_fusion.own_kv_ref, bf16[512,2048]{1,0:T(8,128)(2,1)} %fusion.4.normed_ref, ...), custom_call_target="tpu_custom_call" | custom-call | tf_op jit(solution)/shard_map/fused/pallas_call | solution.py:476
  170.7 1.7 copy.38
  172.4 1.6 copy.39
  (17 shorter events, 0.2 us)
Async XLA Ops:
  0.6 10.5 %copy-start = (bf16[512,96]{0,1:T(8,128)(2,1)S(1)}, bf16[512,96]{0,1:T(8,128)(2,1)}, u32[]{:S(2)}) copy-start(bf16[512,96]{0,1:T(8,128)(2,1)} %param.23) | copy-start | bytes 294916
  0.6 5.9 %copy-start.1 = (bf16[512,2048]{1,0:T(8,128)(2,1)S(1)}, bf16[512,2048]{1,0:T(8,128)(2,1)}, u32[]{:S(2)}) copy-start(bf16[512,2048]{1,0:T(8,128)(2,1)} %param.26) | copy-start | bytes 6291460
  4.5 2.8 %copy-start.2 = (bf16[1024,512]{1,0:T(8,128)(2,1)S(1)}, bf16[1024,512]{1,0:T(8,128)(2,1)}, u32[]{:S(2)}) copy-start(bf16[1024,512]{1,0:T(8,128)(2,1)} %param.18) | copy-start | bytes 3145732
  6.5 1.1 copy-start.3
  6.6 3.0 %copy-start.4 = (bf16[1024,32]{0,1:T(8,128)(2,1)S(1)}, bf16[1024,32]{0,1:T(8,128)(2,1)}, u32[]{:S(2)}) copy-start(bf16[1024,32]{0,1:T(8,128)(2,1)} %param.20) | copy-start | bytes 196612
  6.6 3.0 %copy-start.6 = (bf16[256,128]{1,0:T(8,128)(2,1)S(1)}, bf16[256,128]{1,0:T(8,128)(2,1)}, u32[]{:S(2)}) copy-start(bf16[256,128]{1,0:T(8,128)(2,1)} %param.24) | copy-start | bytes 196612
  6.6 3.0 %copy-start.8 = (f32[256]{0:T(256)S(1)}, f32[256]{0:T(256)}, u32[]{:S(2)}) copy-start(f32[256]{0:T(256)} %param.22) | copy-start | bytes 3076
  7.3 3.9 %copy-start.7 = (f32[512]{0:T(512)S(1)}, f32[512]{0:T(512)}, u32[]{:S(2)}) copy-start(f32[512]{0:T(512)} %param.21) | copy-start | bytes 6148
  11.1 2.4 %copy-start.5 = (f32[2048]{0:T(1024)S(1)}, f32[2048]{0:T(1024)}, u32[]{:S(2)}) copy-start(f32[2048]{0:T(1024)} %param.27) | copy-start | bytes 24580

commit v3 on v2

--- a/solution.py
+++ b/solution.py
@@ -63,10 +63,11 @@
 def fused_kernel(
     ep_count,
     z_count,
-    outgoing_ref,
+    select_ref,
     q_ref,
     own_kv_ref,
-    normed_ref,
+    input_ref,
+    gain_ref,
     gate_ref,
     up_ref,
     down_ref,
@@ -78,6 +79,7 @@
     wout_ref,
     mixed_ref,
     moe_ref,
+    outgoing,
     recv_a,
     buf_x,
     buf_p,
@@ -122,7 +124,7 @@
     steps = half_ring - 1
     slots = ep_count * CAP
     rows = slots + MOE_DEV
-    width = normed_ref.shape[1]
+    width = input_ref.shape[1]
     score_rows = NOPE + ROPE_DIM
     length = q_ref.shape[1]
     tiles = length // QTILE
@@ -132,6 +134,9 @@
     r_half = rows // 2
     r_cols = width // 2
     h_half = VDIM // 2
+    k_half = (score_rows + VDIM) // 2
+    side_x = 4
+    at_y, at_x = lax.div(ep, side_x), lax.rem(ep, side_x)
 
     def around(offset):
         return lax.rem(z + offset + 2 * z_count, z_count)
@@ -154,6 +159,21 @@
             return carry
 
         lax.fori_loop(low, high, run, 0)
+
+    def own_rows(first, count):
+        return layer_scale(input_ref[pl.ds(first, count), :], gain_ref[...])
+
+    kv[ep] = own_kv_ref[...]
+    outgoing[...] = (
+        lax.dot_general(
+            select_ref[...],
+            own_rows(tp * MOE_DEV, MOE_DEV),
+            (((0,), (0,)), ((), ())),
+            preferred_element_type=f32,
+        )
+        .reshape(ep_count, PAD, width)
+        .astype(bf16)
+    )
 
     barrier = pltpu.get_barrier_semaphore()
     loop(1, ep_count, lambda d: pl.semaphore_signal(
@@ -164,30 +184,74 @@
 
     def a_copy(d):
         there = lax.rem(ep + d, ep_count)
-        return remote(outgoing_ref.at[there], recv_a.at[ep], a_send.at[d], a_recv.at[d], at_ep(d))
+        return remote(outgoing.at[there], recv_a.at[ep], a_send.at[d], a_recv.at[d], at_ep(d))
 
     def a_arrival(d):
         source = lax.rem(ep - d + ep_count, ep_count)
-        return remote(outgoing_ref.at[ep], recv_a.at[source], a_send.at[d], a_recv.at[d], at_ep(d))
-
-    def k_copy(d):
-        return remote(own_kv_ref, kv.at[ep], k_send.at[d], k_recv.at[d], at_ep(d))
-
-    def k_arrival(d):
-        source = lax.rem(ep - d + ep_count, ep_count)
-        return remote(own_kv_ref, kv.at[source], k_send.at[d], k_recv.at[d], at_ep(d))
+        return remote(outgoing.at[ep], recv_a.at[source], a_send.at[d], a_recv.at[d], at_ep(d))
 
     def guarded(test, act):
         @pl.when(test)
         def _():
             act()
 
+    def k_copy(origin, half, way):
+        place = (
+            at_y * side_x + lax.rem(at_x + 1, side_x),
+            at_y * side_x + lax.rem(at_x + side_x - 1, side_x),
+            lax.rem(ep + side_x, ep_count),
+            lax.rem(ep + ep_count - side_x, ep_count),
+        )[way]
+        part = kv.at[origin, half * k_half : (half + 1) * k_half]
+        return remote(part, part, k_send.at[origin, half, way], k_recv.at[origin, half], {"ep": place})
+
+    def k_place(origin):
+        from_y, from_x = lax.div(origin, side_x), lax.rem(origin, side_x)
+        return from_y, from_x, lax.rem(at_x - from_x + side_x, side_x)
+
+    def k_pass(origin, act):
+        from_y, from_x, apart = k_place(origin)
+        odd = lax.rem(from_x, 2)
+        same_row, same_column = at_y == from_y, apart == 0
+        both, either = jnp.logical_and, jnp.logical_or
+        right = either(same_column, both(apart == 1, odd == 0))
+        left = either(same_column, both(apart == side_x - 1, odd == 1))
+        down = either(both(same_row, at_y < side_x - 1), both(from_y == 1, at_y == 2))
+        up = both(from_y == 0, either(at_y == 0, at_y == side_x - 1))
+        ways = (
+            (both(right, same_row), both(left, same_row), down, up),
+            (right, left, both(down, same_column), both(up, same_column)),
+        )
+        for half in range(2):
+            for way in range(4):
+                guarded(ways[half][way], lambda: act(k_copy(origin, half, way)))
+
+    def k_stage(stage):
+        def take(origin):
+            from_y, from_x, apart = k_place(origin)
+            far = jnp.logical_or(
+                jnp.logical_and(from_y == 0, at_y == 2), jnp.logical_and(from_y == 1, at_y == 3)
+            )
+            hops = jnp.minimum(apart, side_x - apart) + jnp.where(
+                from_y == at_y, 0, jnp.where(far, 2, 1)
+            )
+
+            def act():
+                for half in range(2):
+                    k_copy(origin, half, 0).wait_recv()
+                k_pass(origin, lambda copy: copy.start())
+
+            guarded(jnp.logical_and(from_y <= at_y, hops == stage), act)
+
+        loop(0, ep_count, take)
+
     loop(1, ep_count, lambda d: a_copy(d).start())
-    loop(1, ep_count, lambda d: guarded(ep + d < ep_count, lambda: k_copy(d).start()))
-    recv_a[ep] = outgoing_ref[ep]
+    k_pass(ep, lambda copy: copy.start())
+    recv_a[ep] = outgoing[ep]
+
 
     def shared_rows(first, count):
-        x = normed_ref[pl.ds(first * count * 2 * MOE_DEV, count * 2 * MOE_DEV), :]
+        x = own_rows(first * count * 2 * MOE_DEV, count * 2 * MOE_DEV)
         hidden = jax.nn.silu(jnp.dot(x, sgate_ref[...], preferred_element_type=f32))
         hidden = (hidden * jnp.dot(x, sup_ref[...], preferred_element_type=f32)).astype(bf16)
         part = jnp.dot(hidden, sdown_ref[...], preferred_element_type=f32).astype(bf16)
@@ -319,22 +383,37 @@
         acc_t[tile] = acc_t[tile] * fade + attended
         m_t[tile] = new_max
 
-    def earlier_block(d):
-        def act():
-            k_arrival(d).wait_recv()
-            for tile in range(tiles):
-                visit(kv.at[ep - d], tile, length, False)
-
-        guarded(d <= ep, act)
-
-    early = 2 * steps
+    def whole_block(origin):
+        for tile in range(tiles):
+            visit(kv.at[origin], tile, length, False)
+
+    def near_block(which):
+        origin = ep - side_x + jnp.where(
+            which == 1,
+            side_x - 1,
+            lax.rem(at_x + jnp.where(which == 2, 3, jnp.where(which == 3, 1, 0)), side_x) - at_x,
+        )
+        present = jnp.where(which == 1, at_x, at_y) > 0
+        guarded(present, lambda: whole_block(origin))
+
+    far_rows = side_x * jnp.maximum(at_y - 1, 0)
+    far_count = far_rows + jnp.minimum(at_y, 1) + jnp.maximum(at_x - 1, 0)
 
     def part_block(unit):
-        d = early + 1 + lax.div(unit, 2)
+        at = lax.div(unit, 2)
         which = lax.rem(unit, 2)
-        guarded(which == 0, lambda: k_arrival(d).wait_recv())
+        row = at_y * side_x
+        beside = row - side_x + lax.rem(at_x + 2, side_x)
+        after = at - far_rows
+        origin = jnp.where(
+            after < 0,
+            at,
+            jnp.where(
+                jnp.logical_and(after == 0, at_y > 0), beside, row + after - jnp.minimum(at_y, 1)
+            ),
+        )
         for tile in range(tiles // 2):
-            visit(kv.at[ep - d], which * (tiles // 2) + tile, length, False)
+            visit(kv.at[origin], which * (tiles // 2) + tile, length, False)
 
     begin_gather(x_ring, x_hand)
     for tile in range(tiles):
@@ -347,7 +426,8 @@
         for side in range(2):
             take_hand(x_hand, offset_of(side, step))
         loop(0, 2, lambda side: expert(lax.rem(step * (2 * side - 1) + z_count, z_count)))
-        loop(2 * step - 1, 2 * step + 1, earlier_block)
+        k_stage(step)
+        guarded(step > 1, lambda: loop(2 * step - 4, 2 * step - 2, near_block))
         loop(0, 2, lambda side: pair_sum(lax.rem(step * (2 * side - 1) + z_count, z_count)))
 
     loop(1, half_ring, gather_step)
@@ -366,9 +446,12 @@
     take_hand(x_hand, half_ring)
     expert(half_ring)
     pair_sum(half_ring)
+    loop(half_ring, 5, k_stage)
+    if half_ring < 4:
+        loop(2 * half_ring - 4, 4, near_block)
 
     events = 4 * (z_count - 2)
-    units = 2 * jnp.maximum(ep - early, 0)
+    units = 2 * far_count
 
     def sum_event(event):
         step = lax.div(event, 4) + 1
@@ -434,7 +517,13 @@
 
     loop(1, ep_count, lambda d: a_copy(d).wait_send())
     loop(1, ep_count, lambda d: b_copy(d).wait_send())
-    loop(1, ep_count, lambda d: guarded(ep + d < ep_count, lambda: k_copy(d).wait_send()))
+    loop(
+        0,
+        ep_count,
+        lambda origin: guarded(
+            lax.div(origin, side_x) <= at_y, lambda: k_pass(origin, lambda copy: copy.wait_send())
+        ),
+    )
 
     def left(step):
         for half in range(2):
@@ -483,6 +572,7 @@
         out_specs=(pl.BlockSpec(memory_space=pltpu.VMEM),) * 2,
         scratch_shapes=[
             vmem((ep_count, PAD, width), bf16),
+            vmem((ep_count, PAD, width), bf16),
             vmem((z_count, 2, slots, width), bf16),
             vmem((z_count, 2, rows, width), bf16),
             vmem((z_count, rows, width), bf16),
@@ -499,8 +589,8 @@
             vmem((tiles, VDIM, QTILE), f32),
             dma((ep_count,)),
             dma((ep_count,)),
-            dma((ep_count,)),
-            dma((ep_count,)),
+            dma((ep_count, 2, 4)),
+            dma((ep_count, 2)),
             dma((2, half_ring + 1, 2)),
             dma((2, half_ring + 1, 2)),
             dma((z_count, 2)),
@@ -552,8 +642,6 @@
     top_count = routes.shape[1]
 
     own_block = lax.axis_index("tp")
-    own_input = lax.dynamic_slice_in_dim(moe_input, own_block * MOE_DEV, MOE_DEV, 0)
-    own_normed = layer_scale(own_input, moe_gain)
     own_routes = lax.dynamic_slice_in_dim(routes, own_block * MOE_DEV, MOE_DEV, 0)
     own_weight = lax.dynamic_slice_in_dim(route_weight, own_block * MOE_DEV, MOE_DEV, 0)
     experts = jnp.arange(ep_count, dtype=jnp.int32)
@@ -569,11 +657,6 @@
     weight_of = jnp.sum(named * own_weight[:, :, None], 1)
     combine = (taken * weight_of[:, :, None]).reshape(MOE_DEV, ep_count * PAD)
     select = taken.reshape(MOE_DEV, ep_count * PAD).astype(bf16)
-    outgoing = (
-        lax.dot_general(select, own_normed, (((0,), (0,)), ((), ())), preferred_element_type=f32)
-        .astype(bf16)
-        .reshape(ep_count, PAD, width)
-    )
     positions = own_index * row_count + jnp.arange(row_count, dtype=jnp.int32)
     cosine_table, sine_table = rotary_tables(positions)
     q_normed = rms_scale(q_latent, q_gain)
@@ -589,7 +672,6 @@
         w_keyval, kv_normed, (((0,), (1,)), ((), ())), preferred_element_type=f32
     ).astype(bf16)
     own_keyvals = jnp.concatenate([expanded[:NOPE], key_rotated, expanded[NOPE:]], 0)
-    normed = layer_scale(moe_input, moe_gain)
     combine_high = combine.astype(bf16)
     combine_low = (combine - combine_high.astype(f32)).astype(bf16)
     mixed, moe_out = fused(
@@ -597,10 +679,11 @@
         tp_count,
         width,
         (
-            outgoing,
+            select,
             queries,
             own_keyvals,
-            normed,
+            moe_input,
+            moe_gain.reshape(1, width),
             expert_gate[0],
             expert_up[0],
             expert_down[0],

time: 174 us -> 149 us (0.86)
  the two profiles are of different devices: /device:TPU:19 before, /device:TPU:27 now
where the time goes in v3:
time: 149 us; the launch traced here: 147 us
  Pallas kernels  133 us (89%)
  other arithmetic  5.63 us (4%)
  local copies, waits for them, and re-layouts  5.19 us (3%)
  matrix products  2.34 us (2%)
    pallas_call x1, Pallas kernels, fused(): pl.pallas_call(functools.partial(fused_kernel, ep_count, z_count), out_sh...  133 us
    unnamed x10, local copies, waits for them, and re-layouts  3.27 us

profile of v3, /device:TPU:27, one launch (start us, length us, event | category | flops | bytes accessed | tf_op | source)
XLA Modules:
  0.0 147.3 jit_solution(14782962396443476572)
XLA Ops:
  0.6 0.0 copy-start
  0.7 0.8 constant_dynamic-slice_fusion
  1.4 0.7 constant_dynamic-slice_fusion.1
  2.2 0.1 copy.30
  2.3 0.1 copy.29
  2.4 0.1 fusion.29
  2.5 0.1 copy.28
  2.6 0.1 eq.40
  2.7 0.6 subtract_convert_fusion
  3.3 0.6 fusion.30
  3.9 0.8 convert_bitcast_fusion
  4.8 0.0 copy-start.1
  4.8 1.6 %fusion = f32[1024]{0:T(1024)S(1)} fusion(bf16[1024,512]{1,0:T(8,128)(2,1)} %param.18), kind=kLoop, calls=%fused_computation.2 | loop fusion | flops 1571840 | bytes 1052672 | tf_op jit(solution)/shard_map/reduce_sum | solution.py:28
  6.4 0.0 copy-start.2
  6.4 0.0 copy-start.3
  6.4 0.0 copy-done
  6.4 1.8 %convolution_bitcast_fusion = f32[96,1024]{1,0:T(8,128)S(1)} fusion(bf16[512,96]{0,1:T(8,128)(2,1)S(1)} %copy-done, bf16[1024,512]{1,0:T(8,128)(2,1)} %param.18, f32[512]{0:T(512)} %param.21, f32[1024]{0:T(1024)S(1)} %add_rsqrt_fusion.1), kind=kOutput, calls=%fused_computation.8 | convolution fusion | flops 102760448 | bytes 1546240 | tf_op jit(solution)/shard_map/dot_general | solution.py:665
  8.2 0.3 fusion.26
  8.6 0.7 pad_maximum_fusion.1.q_ref
  9.3 0.0 copy-done.1
  9.3 0.2 fusion.4
  9.5 0.0 copy-done.2
  9.5 0.0 copy-done.3
  9.5 0.4 fusion.3
  10.0 0.7 pad_maximum_fusion.own_kv_ref
  10.7 133.4 %fused.1 = (bf16[1024,128]{1,0:T(8,128)(2,1)}, bf16[32,2048]{1,0:T(8,128)(2,1)}) custom-call(bf16[32,128]{1,0:T(8,128)(2,1)} %get-tuple-element.15.select_ref, bf16[96,1024]{1,0:T(8,128)(2,1)} %pad_maximum_fusion.1.q_ref, bf16[160,1024]{1,0:T(8,128)(2,1)} %pad_maximum_fusion.own_kv_ref, bf16[512,2048]{1,0:T(8,128)(2,1)} %input_ref.1, f32[1,2048]{1,0:T(1,128)} %bitcast.22, ...), custom_call_target="tpu_custom_call" | custom-call | tf_op jit(solution)/shard_map/fused/pallas_call | solution.py:565
  144.1 1.7 %copy.33 = bf16[1024,128]{1,0:T(8,128)(2,1)} copy(bf16[1024,128]{1,0:T(8,128)(2,1)} %get-tuple-element.18) | data formatting | bytes 524288
  145.8 1.6 %copy.34 = bf16[32,2048]{1,0:T(8,128)(2,1)} copy(bf16[32,2048]{1,0:T(8,128)(2,1)} %get-tuple-element.19) | data formatting | bytes 262144
  (12 shorter events, 0.1 us)
Async XLA Ops:
  0.6 5.8 %copy-start = (bf16[512,96]{0,1:T(8,128)(2,1)S(1)}, bf16[512,96]{0,1:T(8,128)(2,1)}, u32[]{:S(2)}) copy-start(bf16[512,96]{0,1:T(8,128)(2,1)} %param.23) | copy-start | bytes 294916
  4.8 4.5 %copy-start.1 = (bf16[1024,256]{1,0:T(8,128)(2,1)S(1)}, bf16[1024,256]{1,0:T(8,128)(2,1)}, u32[]{:S(2)}) copy-start(bf16[1024,256]{1,0:T(8,128)(2,1)} %param.19) | copy-start | bytes 1572868
  6.4 3.1 %copy-start.2 = (bf16[256,128]{1,0:T(8,128)(2,1)S(1)}, bf16[256,128]{1,0:T(8,128)(2,1)}, u32[]{:S(2)}) copy-start(bf16[256,128]{1,0:T(8,128)(2,1)} %param.24) | copy-start | bytes 196612
  6.4 3.1 %copy-start.3 = (f32[256]{0:T(256)S(1)}, f32[256]{0:T(256)}, u32[]{:S(2)}) copy-start(f32[256]{0:T(256)} %param.22) | copy-start | bytes 3076

commit v4 on v3

--- a/solution.py
+++ b/solution.py
@@ -18,7 +18,7 @@
 layer_eps = 1e-05
 rotary_base = 10000.0
 floor_value = -1e30
-QTILE = 256
+QTILE = 512
 LOG2E = 1.4426950408889634
 
 
@@ -58,27 +58,46 @@
 
 
 MESH = pl.DeviceIdType.MESH
+HELD = 10
 
 
 def fused_kernel(
     ep_count,
     z_count,
-    select_ref,
-    q_ref,
-    own_kv_ref,
+    cosine_ref,
+    sine_ref,
+    rope_ref,
+    q_gain_ref,
+    kv_gain_ref,
+    gain_ref,
+    routes_ref,
+    route_weight_ref,
+    w_query_ref,
+    w_keyval_ref,
+    input_hbm,
+    kv_latent_hbm,
+    q_latent_hbm,
+    sgate_hbm,
+    sup_hbm,
+    sdown_hbm,
+    gate_hbm,
+    up_hbm,
+    down_hbm,
+    wout_hbm,
+    mixed_ref,
+    moe_ref,
+    own_ref,
     input_ref,
-    gain_ref,
+    kv_latent_ref,
+    q_latent_ref,
+    sgate_ref,
+    sup_ref,
+    sdown_ref,
     gate_ref,
     up_ref,
     down_ref,
-    sgate_ref,
-    sup_ref,
-    sdown_ref,
-    chigh_ref,
-    clow_ref,
     wout_ref,
-    mixed_ref,
-    moe_ref,
+    l_send,
     outgoing,
     recv_a,
     buf_x,
@@ -126,7 +145,7 @@
     rows = slots + MOE_DEV
     width = input_ref.shape[1]
     score_rows = NOPE + ROPE_DIM
-    length = q_ref.shape[1]
+    length = rope_ref.shape[1]
     tiles = length // QTILE
     scale = float(score_rows) ** (-0.5) * LOG2E
     partner = {"tp": z * 2 + other}
@@ -160,26 +179,74 @@
 
         lax.fori_loop(low, high, run, 0)
 
-    def own_rows(first, count):
-        return layer_scale(input_ref[pl.ds(first, count), :], gain_ref[...])
-
-    kv[ep] = own_kv_ref[...]
-    outgoing[...] = (
-        lax.dot_general(
-            select_ref[...],
-            own_rows(tp * MOE_DEV, MOE_DEV),
-            (((0,), (0,)), ((), ())),
-            preferred_element_type=f32,
-        )
-        .reshape(ep_count, PAD, width)
-        .astype(bf16)
-    )
-
     barrier = pltpu.get_barrier_semaphore()
     loop(1, ep_count, lambda d: pl.semaphore_signal(
         barrier, inc=1, device_id=at_ep(d), device_id_type=MESH))
     for device in (at_z(1), at_z(-1), partner):
         pl.semaphore_signal(barrier, inc=1, device_id=device, device_id_type=MESH)
+
+    first_own = pl.multiple_of(tp * MOE_DEV, MOE_DEV)
+    fetches = [
+        pltpu.make_async_copy(source, target, l_send.at[at])
+        for at, (source, target) in enumerate(
+            (
+                (input_hbm.at[pl.ds(first_own, MOE_DEV)], own_ref),
+                (kv_latent_hbm, kv_latent_ref),
+                (q_latent_hbm, q_latent_ref),
+                (input_hbm, input_ref),
+                (sgate_hbm, sgate_ref),
+                (sup_hbm, sup_ref),
+                (sdown_hbm, sdown_ref),
+                (gate_hbm, gate_ref),
+                (up_hbm, up_ref),
+                (down_hbm, down_ref),
+                (wout_hbm, wout_ref),
+            )
+        )
+    ]
+    for fetch in fetches:
+        fetch.start()
+
+    lanes = (MOE_DEV, ep_count * PAD)
+    expert_at = lax.div(lax.broadcasted_iota(jnp.int32, lanes, 1), PAD).astype(f32)
+    slot_at = lax.rem(lax.broadcasted_iota(jnp.int32, lanes, 1), PAD).astype(f32)
+    tokens = (MOE_DEV, routes_ref.shape[1])
+    own_at = lax.broadcasted_iota(jnp.int32, tokens, 1) == (
+        lax.broadcasted_iota(jnp.int32, tokens, 0) + tp * MOE_DEV
+    )
+
+    def own_column(row):
+        return jnp.sum(jnp.where(own_at, row.astype(f32), 0.0), 1, keepdims=True)
+
+    named = [
+        (own_column(routes_ref[k : k + 1, :]) == expert_at).astype(f32)
+        for k in range(routes_ref.shape[0])
+    ]
+    in_row = sum(named)
+    square = (MOE_DEV, MOE_DEV)
+    before = (
+        lax.broadcasted_iota(jnp.int32, square, 1) < lax.broadcasted_iota(jnp.int32, square, 0)
+    ).astype(bf16)
+    rank = jnp.dot(before, in_row.astype(bf16), preferred_element_type=f32)
+    taken = jnp.where(rank == slot_at, in_row, 0.0)
+    weight_of = sum(
+        named[k] * own_column(route_weight_ref[k : k + 1, :]) for k in range(len(named))
+    )
+    combine = taken * weight_of
+    combine_high = combine.astype(bf16)
+    combine_low = (combine - combine_high.astype(f32)).astype(bf16)
+
+    fetches[0].wait()
+    outgoing[...] = (
+        lax.dot_general(
+            taken.astype(bf16),
+            layer_scale(own_ref[...], gain_ref[...]),
+            (((0,), (0,)), ((), ())),
+            preferred_element_type=f32,
+        )
+        .reshape(ep_count, PAD, width)
+        .astype(bf16)
+    )
     pl.semaphore_wait(barrier, ep_count + 2)
 
     def a_copy(d):
@@ -246,12 +313,37 @@
         loop(0, ep_count, take)
 
     loop(1, ep_count, lambda d: a_copy(d).start())
-    k_pass(ep, lambda copy: copy.start())
     recv_a[ep] = outgoing[ep]
 
+    transposed = (((1,), (1,)), ((), ()))
+    fetches[1].wait()
+    kv_normed = rms_scale(kv_latent_ref[...], kv_gain_ref[...])
+    expanded = lax.dot_general(
+        w_keyval_ref[...].T, kv_normed, transposed, preferred_element_type=f32
+    ).astype(bf16)
+    kv[ep, 0:NOPE] = expanded[0:NOPE]
+    kv[ep, NOPE:score_rows] = rotate_rows(
+        rope_ref[...].astype(f32), cosine_ref[...], sine_ref[...]
+    ).astype(bf16)
+    kv[ep, score_rows:] = expanded[NOPE:]
+    fetches[2].wait()
+    q_normed = rms_scale(q_latent_ref[...], q_gain_ref[...])
+    projected = lax.dot_general(w_query_ref[...], q_normed, transposed, preferred_element_type=f32)
+    queries = jnp.concatenate(
+        [
+            projected[0:NOPE],
+            rotate_rows(projected[NOPE:], cosine_ref[...], sine_ref[...]),
+        ],
+        0,
+    ).astype(bf16)
+    for tile in range(tiles):
+        q_t[tile] = queries[:, tile * QTILE : (tile + 1) * QTILE]
+
 
     def shared_rows(first, count):
-        x = own_rows(first * count * 2 * MOE_DEV, count * 2 * MOE_DEV)
+        x = layer_scale(
+            input_ref[pl.ds(first * count * 2 * MOE_DEV, count * 2 * MOE_DEV), :], gain_ref[...]
+        )
         hidden = jax.nn.silu(jnp.dot(x, sgate_ref[...], preferred_element_type=f32))
         hidden = (hidden * jnp.dot(x, sup_ref[...], preferred_element_type=f32)).astype(bf16)
         part = jnp.dot(hidden, sdown_ref[...], preferred_element_type=f32).astype(bf16)
@@ -260,11 +352,11 @@
                 begin = (at * 2 + side) * MOE_DEV
                 buf_p[first * count + at, side, slots:rows, :] = part[begin : begin + MOE_DEV]
 
+    for fetch in fetches[3:7]:
+        fetch.wait()
     per_call = 2
     loop(0, z_count // per_call, lambda first: shared_rows(first, per_call))
 
-    for tile in range(tiles):
-        q_t[tile] = q_ref[:, tile * QTILE : (tile + 1) * QTILE]
     m_t[...] = jnp.full_like(m_t, floor_value)
     l_t[...] = jnp.zeros_like(l_t)
     acc_t[...] = jnp.zeros_like(acc_t)
@@ -416,22 +508,27 @@
             visit(kv.at[origin], which * (tiles // 2) + tile, length, False)
 
     begin_gather(x_ring, x_hand)
+    k_pass(ep, lambda copy: copy.start())
     for tile in range(tiles):
-        visit(own_kv_ref, tile, (tile + 1) * QTILE, True)
-    take_hand(x_hand, 0)
-    expert(0)
+        visit(kv.at[ep], tile, (tile + 1) * QTILE, True)
+    for fetch in fetches[7:10]:
+        fetch.wait()
+
+    def hidden_work(offset):
+        take_hand(x_hand, offset)
+        expert(offset)
+
+    def beside(step, side):
+        return lax.rem(step * (2 * side - 1) + z_count, z_count)
 
     def gather_step(step):
         pass_on(x_ring, x_hand, step)
-        for side in range(2):
-            take_hand(x_hand, offset_of(side, step))
-        loop(0, 2, lambda side: expert(lax.rem(step * (2 * side - 1) + z_count, z_count)))
+        loop(0, jnp.minimum(step, 2), lambda side: hidden_work(beside(step - 1, side)))
         k_stage(step)
         guarded(step > 1, lambda: loop(2 * step - 4, 2 * step - 2, near_block))
-        loop(0, 2, lambda side: pair_sum(lax.rem(step * (2 * side - 1) + z_count, z_count)))
+        loop(0, jnp.minimum(step - 1, 2), lambda side: pair_sum(beside(step - 2, side)))
 
     loop(1, half_ring, gather_step)
-    pass_last(x_ring, x_hand)
 
     def r_copy(step, side, half, chunk):
         return remote(
@@ -439,14 +536,20 @@
             r_send.at[step, side, half], r_recv.at[step, side, half], at_z(1 - 2 * side),
         )
 
-    for half in range(2):
-        for side in range(2):
-            r_copy(0, side, half, around(2 * side - 1)).start()
-    pair_sum(0)
-    take_hand(x_hand, half_ring)
-    expert(half_ring)
-    pair_sum(half_ring)
+    def begin_sums():
+        for half in range(2):
+            for side in range(2):
+                r_copy(0, side, half, around(2 * side - 1)).start()
+
+    if half_ring >= 4:
+        begin_sums()
+    loop(0, 2, lambda side: hidden_work(beside(half_ring - 1, side)))
+    pass_last(x_ring, x_hand)
     loop(half_ring, 5, k_stage)
+    hidden_work(half_ring)
+    loop(half_ring - 2, min(half_ring + 3, z_count), pair_sum)
+    if half_ring < 4:
+        begin_sums()
     if half_ring < 4:
         loop(2 * half_ring - 4, 4, near_block)
 
@@ -502,18 +605,19 @@
     loop(1, ep_count, lambda d: b_arrival(d).wait_recv())
     returned = recv_b[...].astype(f32).reshape(ep_count * PAD, width).astype(bf16)
     moe_ref[...] = (
-        jnp.dot(chigh_ref[...], returned, preferred_element_type=f32)
-        + jnp.dot(clow_ref[...], returned, preferred_element_type=f32)
+        jnp.dot(combine_high, returned, preferred_element_type=f32)
+        + jnp.dot(combine_low, returned, preferred_element_type=f32)
         + final[slots:rows, :]
-    ).astype(bf16)
+    )
 
     loop(0, z_count, lambda offset: take_hand(h_hand, offset))
+    fetches[10].wait()
     mixed_ref[...] = lax.dot_general(
         heads[...].reshape(2 * z_count * VDIM, length),
         wout_ref[...],
         (((0,), (0,)), ((), ())),
         preferred_element_type=f32,
-    ).astype(bf16)
+    )
 
     loop(1, ep_count, lambda d: a_copy(d).wait_send())
     loop(1, ep_count, lambda d: b_copy(d).wait_send())
@@ -558,19 +662,24 @@
     half_ring = z_count // 2
     slots = ep_count * CAP
     rows = slots + MOE_DEV
-    score_rows, length = operands[1].shape
+    score_rows, length = NOPE + ROPE_DIM, operands[2].shape[1]
+    staged = operands[HELD:]
     tiles = length // QTILE
     dma = pltpu.SemaphoreType.DMA
     vmem = pltpu.VMEM
     return pl.pallas_call(
         functools.partial(fused_kernel, ep_count, z_count),
         out_shape=(
-            jax.ShapeDtypeStruct((length, operands[-1].shape[1]), bf16),
-            jax.ShapeDtypeStruct((MOE_DEV, width), bf16),
+            jax.ShapeDtypeStruct((length, operands[-1].shape[1]), f32),
+            jax.ShapeDtypeStruct((MOE_DEV, width), f32),
         ),
-        in_specs=[pl.BlockSpec(memory_space=pltpu.VMEM)] * len(operands),
+        in_specs=[pl.BlockSpec(memory_space=pltpu.VMEM)] * HELD
+        + [pl.BlockSpec(memory_space=pl.ANY)] * len(staged),
         out_specs=(pl.BlockSpec(memory_space=pltpu.VMEM),) * 2,
         scratch_shapes=[
+            vmem((MOE_DEV, width), bf16),
+            *[vmem(array.shape, bf16) for array in staged],
+            dma((len(staged) + 1,)),
             vmem((ep_count, PAD, width), bf16),
             vmem((ep_count, PAD, width), bf16),
             vmem((z_count, 2, slots, width), bf16),
@@ -633,69 +742,42 @@
     shared_up,
     shared_down,
 ):
-    f32, bf16 = jnp.float32, jnp.bfloat16
     row_count = q_latent.shape[0]
     own_index = lax.axis_index("ep")
     ep_count = lax.axis_size("ep")
     tp_count = lax.axis_size("tp")
     width = moe_input.shape[1]
-    top_count = routes.shape[1]
-
-    own_block = lax.axis_index("tp")
-    own_routes = lax.dynamic_slice_in_dim(routes, own_block * MOE_DEV, MOE_DEV, 0)
-    own_weight = lax.dynamic_slice_in_dim(route_weight, own_block * MOE_DEV, MOE_DEV, 0)
-    experts = jnp.arange(ep_count, dtype=jnp.int32)
-    named = (own_routes[:, :, None] == experts).astype(f32)
-    in_row = jnp.sum(named, 1)
-    token_at = jnp.arange(MOE_DEV)
-    before = (token_at[None, :] < token_at[:, None]).astype(f32)
-    rank = jnp.dot(before, in_row, preferred_element_type=f32)
-    slot_at = jnp.arange(PAD, dtype=f32)
-    taken = jnp.where(
-        (in_row[:, :, None] > 0) & (rank[:, :, None] == slot_at), 1.0, 0.0
-    )
-    weight_of = jnp.sum(named * own_weight[:, :, None], 1)
-    combine = (taken * weight_of[:, :, None]).reshape(MOE_DEV, ep_count * PAD)
-    select = taken.reshape(MOE_DEV, ep_count * PAD).astype(bf16)
+
     positions = own_index * row_count + jnp.arange(row_count, dtype=jnp.int32)
     cosine_table, sine_table = rotary_tables(positions)
-    q_normed = rms_scale(q_latent, q_gain)
-    kv_normed = rms_scale(kv_latent, kv_gain)
-    key_rotated = rotate_rows(rope_key.T.astype(f32), cosine_table, sine_table).astype(bf16)
-    projected = lax.dot_general(
-        w_query, q_normed, (((0,), (1,)), ((), ())), preferred_element_type=f32
-    )
-    queries = jnp.concatenate(
-        [projected[:NOPE], rotate_rows(projected[NOPE:], cosine_table, sine_table)], 0
-    ).astype(bf16)
-    expanded = lax.dot_general(
-        w_keyval, kv_normed, (((0,), (1,)), ((), ())), preferred_element_type=f32
-    ).astype(bf16)
-    own_keyvals = jnp.concatenate([expanded[:NOPE], key_rotated, expanded[NOPE:]], 0)
-    combine_high = combine.astype(bf16)
-    combine_low = (combine - combine_high.astype(f32)).astype(bf16)
     mixed, moe_out = fused(
         ep_count,
         tp_count,
         width,
         (
-            select,
-            queries,
-            own_keyvals,
+            cosine_table,
+            sine_table,
+            rope_key.T,
+            q_gain.reshape(1, -1),
+            kv_gain.reshape(1, -1),
+            moe_gain.reshape(1, -1),
+            routes.T,
+            route_weight.T,
+            w_query.T,
+            w_keyval,
             moe_input,
-            moe_gain.reshape(1, width),
+            kv_latent,
+            q_latent,
+            shared_gate,
+            shared_up,
+            shared_down,
             expert_gate[0],
             expert_up[0],
             expert_down[0],
-            shared_gate,
-            shared_up,
-            shared_down,
-            combine_high,
-            combine_low,
             w_output,
         ),
     )
-    return (mixed, moe_out)
+    return (mixed.astype(jnp.bfloat16), moe_out.astype(jnp.bfloat16))
 
 
 def solution(mesh):

time: 149 us -> 132 us (0.89)
  Pallas kernels: 133 us -> 125 us
  local copies, waits for them, and re-layouts: 5.19 us -> 0 us
  matrix products: 2.34 us -> 0 us
    pallas_call x1, Pallas kernels: 133 us -> 125 us  [fused(): pl.pallas_call(functools.partial(fused_kernel, ep_count, z_count), out_sh...]
    unnamed x10 -> x0, local copies, waits for them, and re-layouts: 3.27 us -> none
    dot_general x3 -> x0, matrix products: 2.34 us -> none  [the longest x1 1.78 us: body(): lax.dot_general(w_query, q_normed, (((0,), (1,)), ((), ())), preferred_el...]
    reduce_sum x3 -> x0, other arithmetic: 1.78 us -> none  [the longest x2 1.77 us: rms_scale(): jnp.mean(widened * widened, -1, keepdims=True) + norm_eps]
    dynamic_slice x2 -> x0, local copies, waits for them, and re-layouts: 1.54 us -> none  [the longest x1 0.79 us: body(): lax.dynamic_slice_in_dim(route_weight, own_block * MOE_DEV, MOE_DEV, 0)]
    convert_element_type x3 -> x2, other arithmetic: 2.07 us -> 3.39 us  [body(): return (mixed.astype(jnp.bfloat16), moe_out.astype(jnp.bfloat16))]
where the time goes in v4:
time: 132 us; the launch traced here: 130 us
  Pallas kernels  125 us (95%)
  other arithmetic  4.37 us (3%)
    pallas_call x1, Pallas kernels, fused(): pl.pallas_call(functools.partial(fused_kernel, ep_count, z_count), out_sh...  125 us
    convert_element_type x2, other arithmetic, body(): return (mixed.astype(jnp.bfloat16), moe_out.astype(jnp.bfloat16))  3.39 us

profile of v4, /device:TPU:27, one launch (start us, length us, event | category | flops | bytes accessed | tf_op | source)
XLA Modules:
  0.0 129.9 jit_solution(15327561372499864997)
XLA Ops:
  0.7 1.0 multiply_sine_fusion
  1.6 124.8 %fused.1 = (f32[1024,128]{1,0:T(8,128)}, f32[32,2048]{1,0:T(8,128)}) custom-call(f32[16,1024]{1,0:T(8,128)} %get-tuple-element.7.cosine_ref, f32[16,1024]{1,0:T(8,128)} %get-tuple-element.6.sine_ref, bf16[32,1024]{1,0:T(8,128)(2,1)} %bitcast.14, f32[1,512]{1,0:T(1,128)} %bitcast.18, f32[1,256]{1,0:T(1,128)} %bitcast.19, f32[1,2048]{1,0:T(1,128)} %bitcast.15, ...), custom_call_target="tpu_custom_call" | custom-call | tf_op jit(solution)/shard_map/fused/pallas_call | solution.py:670
  126.5 1.8 %convert_element_type.14 = bf16[1024,128]{1,0:T(8,128)(2,1)} convert(f32[1024,128]{1,0:T(8,128)} %get-tuple-element.4) | non-fusion elementwise | flops 131072 | bytes 786432 | tf_op jit(solution)/shard_map/convert_element_type | solution.py:780
  128.2 1.6 %convert_element_type.15 = bf16[32,2048]{1,0:T(8,128)(2,1)} convert(f32[32,2048]{1,0:T(8,128)} %get-tuple-element.5) | non-fusion elementwise | flops 65536 | bytes 393216 | tf_op jit(solution)/shard_map/convert_element_type | solution.py:780
  (2 shorter events, 0.0 us)

commit v5 on v4

--- a/solution.py
+++ b/solution.py
@@ -13,6 +13,7 @@
 MOE_DEV = 32
 CAP = 6
 PAD = 8
+PACK = 3
 
 norm_eps = 1e-06
 layer_eps = 1e-05
@@ -153,9 +154,13 @@
     r_half = rows // 2
     r_cols = width // 2
     h_half = VDIM // 2
+    fourth = width // 4
     k_half = (score_rows + VDIM) // 2
     side_x = 4
     at_y, at_x = lax.div(ep, side_x), lax.rem(ep, side_x)
+
+    def columns(part):
+        return slice(part * fourth, (part + 1) * fourth)
 
     def around(offset):
         return lax.rem(z + offset + 2 * z_count, z_count)
@@ -210,6 +215,11 @@
     lanes = (MOE_DEV, ep_count * PAD)
     expert_at = lax.div(lax.broadcasted_iota(jnp.int32, lanes, 1), PAD).astype(f32)
     slot_at = lax.rem(lax.broadcasted_iota(jnp.int32, lanes, 1), PAD).astype(f32)
+
+    def tail_slot(part):
+        low = jnp.where(slot_at == CAP, float(part), -1.0)
+        return jnp.where(slot_at == CAP + 1, float(PACK + part), low)
+
     tokens = (MOE_DEV, routes_ref.shape[1])
     own_at = lax.broadcasted_iota(jnp.int32, tokens, 1) == (
         lax.broadcasted_iota(jnp.int32, tokens, 0) + tp * MOE_DEV
@@ -232,21 +242,25 @@
     weight_of = sum(
         named[k] * own_column(route_weight_ref[k : k + 1, :]) for k in range(len(named))
     )
-    combine = taken * weight_of
-    combine_high = combine.astype(bf16)
-    combine_low = (combine - combine_high.astype(f32)).astype(bf16)
+    tails = [jnp.where(rank == tail_slot(part), in_row, 0.0) for part in range(PACK)]
 
     fetches[0].wait()
-    outgoing[...] = (
-        lax.dot_general(
-            taken.astype(bf16),
-            layer_scale(own_ref[...], gain_ref[...]),
-            (((0,), (0,)), ((), ())),
-            preferred_element_type=f32,
-        )
-        .reshape(ep_count, PAD, width)
-        .astype(bf16)
-    )
+    own_normed = layer_scale(own_ref[...], gain_ref[...])
+
+    def placed(chosen, rows_in):
+        return lax.dot_general(
+            chosen.astype(bf16), rows_in, (((0,), (0,)), ((), ())), preferred_element_type=f32
+        )
+
+    for part in range(PACK):
+        outgoing[:, :, columns(part)] = (
+            (
+                placed(taken, own_normed[:, columns(part)])
+                + placed(tails[part], own_normed[:, columns(PACK)])
+            )
+            .reshape(ep_count, PAD, fourth)
+            .astype(bf16)
+        )
     pl.semaphore_wait(barrier, ep_count + 2)
 
     def a_copy(d):
@@ -361,18 +375,27 @@
     l_t[...] = jnp.zeros_like(l_t)
     acc_t[...] = jnp.zeros_like(acc_t)
 
-    def squeeze_rows(shape, slot_dim):
+    def squeeze_rows(shape, slot_dim, part=None):
         slot = lax.broadcasted_iota(jnp.int32, shape, slot_dim)
         place = lax.broadcasted_iota(jnp.int32, shape, 1 - slot_dim)
-        return jnp.where(
-            place == lax.div(slot, CAP) * PAD + lax.rem(slot, CAP), 1.0, 0.0
+        expert, number = lax.div(slot, CAP), lax.rem(slot, CAP)
+        if part is None:
+            return jnp.where(place == expert * PAD + number, 1.0, 0.0).astype(bf16)
+        target = expert * PAD + CAP + lax.div(number, PACK)
+        here = jnp.logical_and(place == target, lax.rem(number, PACK) == part)
+        return jnp.where(here, 1.0, 0.0).astype(bf16)
+
+    loop(1, ep_count, lambda d: a_arrival(d).wait_recv())
+    arrived = recv_a[...].astype(f32).reshape(ep_count * PAD, PACK * fourth).astype(bf16)
+    packed_shape = (slots, ep_count * PAD)
+    last = 0.0
+    for part in range(PACK):
+        piece = arrived[:, columns(part)]
+        buf_x[z, core, :, columns(part)] = jnp.dot(
+            squeeze_rows(packed_shape, 0), piece, preferred_element_type=f32
         ).astype(bf16)
-
-    loop(1, ep_count, lambda d: a_arrival(d).wait_recv())
-    arrived = recv_a[...].astype(f32).reshape(ep_count * PAD, width).astype(bf16)
-    buf_x[z, core] = jnp.dot(
-        squeeze_rows((slots, ep_count * PAD), 0), arrived, preferred_element_type=f32
-    ).astype(bf16)
+        last += jnp.dot(squeeze_rows(packed_shape, 0, part), piece, preferred_element_type=f32)
+    buf_x[z, core, :, columns(PACK)] = last.astype(bf16)
 
     def ring_copy(buf, send, recv, size, side, step, half, origin):
         part = pl.ds(half * size, size)
@@ -524,7 +547,7 @@
     def gather_step(step):
         pass_on(x_ring, x_hand, step)
         loop(0, jnp.minimum(step, 2), lambda side: hidden_work(beside(step - 1, side)))
-        k_stage(step)
+        guarded(step < 3, lambda: k_stage(step))
         guarded(step > 1, lambda: loop(2 * step - 4, 2 * step - 2, near_block))
         loop(0, jnp.minimum(step - 1, 2), lambda side: pair_sum(beside(step - 2, side)))
 
@@ -545,7 +568,10 @@
         begin_sums()
     loop(0, 2, lambda side: hidden_work(beside(half_ring - 1, side)))
     pass_last(x_ring, x_hand)
-    loop(half_ring, 5, k_stage)
+    if half_ring >= 4:
+        k_stage(3)
+    else:
+        loop(half_ring, 4, k_stage)
     hidden_work(half_ring)
     loop(half_ring - 2, min(half_ring + 3, z_count), pair_sum)
     if half_ring < 4:
@@ -555,6 +581,7 @@
 
     events = 4 * (z_count - 2)
     units = 2 * far_count
+    quiet = 4
 
     def sum_event(event):
         step = lax.div(event, 4) + 1
@@ -566,7 +593,10 @@
             buf_s[chunk, side, half].astype(f32) + recv_r[step - 1, side, half].astype(f32)
         ).astype(bf16)
         r_copy(step, side, half, chunk).start()
-        loop(lax.div(event * units, events), lax.div((event + 1) * units, events), part_block)
+        guarded(event == quiet - 1, lambda: k_stage(4))
+        done = jnp.maximum(event - quiet, 0) * units
+        due = jnp.maximum(event + 1 - quiet, 0) * units
+        loop(lax.div(done, events - quiet), lax.div(due, events - quiet), part_block)
 
     loop(0, events, sum_event)
 
@@ -581,12 +611,15 @@
                 buf_s[z, side, half].astype(f32) + recv_r[z_count - 2, side, half].astype(f32)
             )
 
-    spread = jnp.dot(
-        squeeze_rows((ep_count * PAD, slots), 1),
-        final[0:slots, :].astype(bf16),
-        preferred_element_type=f32,
-    )
-    send_b[...] = spread.reshape(ep_count, PAD, width).astype(bf16)
+    sums = final[0:slots, :].astype(bf16)
+    spread_shape = (ep_count * PAD, slots)
+    for part in range(PACK):
+        spread = jnp.dot(
+            squeeze_rows(spread_shape, 1), sums[:, columns(part)], preferred_element_type=f32
+        ) + jnp.dot(
+            squeeze_rows(spread_shape, 1, part), sums[:, columns(PACK)], preferred_element_type=f32
+        )
+        send_b[:, :, columns(part)] = spread.reshape(ep_count, PAD, fourth).astype(bf16)
 
     def b_copy(d):
         there = lax.rem(ep + d, ep_count)
@@ -603,12 +636,22 @@
     pass_last(h_ring, h_hand)
 
     loop(1, ep_count, lambda d: b_arrival(d).wait_recv())
-    returned = recv_b[...].astype(f32).reshape(ep_count * PAD, width).astype(bf16)
-    moe_ref[...] = (
-        jnp.dot(combine_high, returned, preferred_element_type=f32)
-        + jnp.dot(combine_low, returned, preferred_element_type=f32)
-        + final[slots:rows, :]
-    )
+    returned = recv_b[...].astype(f32).reshape(ep_count * PAD, PACK * fourth).astype(bf16)
+
+    def weighed(chosen, rows_in):
+        combine = chosen * weight_of
+        high = combine.astype(bf16)
+        low = (combine - high.astype(f32)).astype(bf16)
+        return jnp.dot(high, rows_in, preferred_element_type=f32) + jnp.dot(
+            low, rows_in, preferred_element_type=f32
+        )
+
+    last = final[slots:rows, columns(PACK)]
+    for part in range(PACK):
+        piece = returned[:, columns(part)]
+        moe_ref[:, columns(part)] = weighed(taken, piece) + final[slots:rows, columns(part)]
+        last += weighed(tails[part], piece)
+    moe_ref[:, columns(PACK)] = last
 
     loop(0, z_count, lambda offset: take_hand(h_hand, offset))
     fetches[10].wait()
@@ -680,8 +723,8 @@
             vmem((MOE_DEV, width), bf16),
             *[vmem(array.shape, bf16) for array in staged],
             dma((len(staged) + 1,)),
-            vmem((ep_count, PAD, width), bf16),
-            vmem((ep_count, PAD, width), bf16),
+            vmem((ep_count, PAD, width // 4 * PACK), bf16),
+            vmem((ep_count, PAD, width // 4 * PACK), bf16),
             vmem((z_count, 2, slots, width), bf16),
             vmem((z_count, 2, rows, width), bf16),
             vmem((z_count, rows, width), bf16),
@@ -690,8 +733,8 @@
             vmem((rows, width), f32),
             vmem((ep_count, score_rows + VDIM, length), bf16),
             vmem((z_count, 2, VDIM, length), bf16),
-            vmem((ep_count, PAD, width), bf16),
-            vmem((ep_count, PAD, width), bf16),
+            vmem((ep_count, PAD, width // 4 * PACK), bf16),
+            vmem((ep_count, PAD, width // 4 * PACK), bf16),
             vmem((tiles, score_rows, QTILE), bf16),
             vmem((tiles, 1, QTILE), f32),
             vmem((tiles, 1, QTILE), f32),

time: 132 us -> 126 us (0.955); the launches traced: 130 us -> 126 us
  Pallas kernels: 125 us -> 121 us
    pallas_call x1, Pallas kernels: 125 us -> 121 us  [fused(): pl.pallas_call(functools.partial(fused_kernel, ep_count, z_count), out_sh...]
where the time goes in v5:
time: 126 us
  Pallas kernels  121 us (96%)
  other arithmetic  4.37 us (3%)
    pallas_call x1, Pallas kernels, fused(): pl.pallas_call(functools.partial(fused_kernel, ep_count, z_count), out_sh...  121 us
    convert_element_type x2, other arithmetic, body(): return (mixed.astype(jnp.bfloat16), moe_out.astype(jnp.bfloat16))  3.39 us

profile of v5, /device:TPU:27, one launch (start us, length us, event | category | flops | bytes accessed | tf_op | source)
XLA Modules:
  0.0 126.1 jit_solution(224197715928456820)
XLA Ops:
  0.7 1.0 multiply_sine_fusion
  1.6 121.1 %fused.1 = (f32[1024,128]{1,0:T(8,128)}, f32[32,2048]{1,0:T(8,128)}) custom-call(f32[16,1024]{1,0:T(8,128)} %get-tuple-element.7.cosine_ref, f32[16,1024]{1,0:T(8,128)} %get-tuple-element.6.sine_ref, bf16[32,1024]{1,0:T(8,128)(2,1)} %bitcast.14, f32[1,512]{1,0:T(1,128)} %bitcast.18, f32[1,256]{1,0:T(1,128)} %bitcast.19, f32[1,2048]{1,0:T(1,128)} %bitcast.15, ...), custom_call_target="tpu_custom_call" | custom-call | tf_op jit(solution)/shard_map/fused/pallas_call | solution.py:713
  122.7 1.8 %convert_element_type.14 = bf16[1024,128]{1,0:T(8,128)(2,1)} convert(f32[1024,128]{1,0:T(8,128)} %get-tuple-element.4) | non-fusion elementwise | flops 131072 | bytes 786432 | tf_op jit(solution)/shard_map/convert_element_type | solution.py:823
  124.5 1.6 %convert_element_type.15 = bf16[32,2048]{1,0:T(8,128)(2,1)} convert(f32[32,2048]{1,0:T(8,128)} %get-tuple-element.5) | non-fusion elementwise | flops 65536 | bytes 393216 | tf_op jit(solution)/shard_map/convert_element_type | solution.py:823
  (2 shorter events, 0.0 us)

commit v6 on v5

--- a/solution.py
+++ b/solution.py
@@ -632,6 +632,38 @@
     loop(1, ep_count, lambda d: b_copy(d).start())
     recv_b[ep] = send_b[ep]
 
+    def all_left(ring, hand):
+        def left(step):
+            for half in range(2):
+                for side in range(2):
+                    ring(side, step, half, z).wait_send()
+
+        def handed(offset):
+            for half in range(2):
+                hand(offset, half, core).wait_send()
+
+        loop(1, half_ring, left)
+        for side in range(2):
+            ring(side, half_ring, side, z).wait_send()
+        loop(0, z_count, handed)
+
+    def summed(step):
+        for half in range(2):
+            for side in range(2):
+                r_copy(step, side, half, z).wait_send()
+
+    loop(1, ep_count, lambda d: a_copy(d).wait_send())
+    loop(
+        0,
+        ep_count,
+        lambda origin: guarded(
+            lax.div(origin, side_x) <= at_y, lambda: k_pass(origin, lambda copy: copy.wait_send())
+        ),
+    )
+    all_left(x_ring, x_hand)
+    loop(0, z_count, lambda offset: p_copy(offset).wait_send())
+    loop(0, z_count - 1, summed)
+
     loop(1, half_ring, lambda step: pass_on(h_ring, h_hand, step))
     pass_last(h_ring, h_hand)
 
@@ -662,41 +694,8 @@
         preferred_element_type=f32,
     )
 
-    loop(1, ep_count, lambda d: a_copy(d).wait_send())
     loop(1, ep_count, lambda d: b_copy(d).wait_send())
-    loop(
-        0,
-        ep_count,
-        lambda origin: guarded(
-            lax.div(origin, side_x) <= at_y, lambda: k_pass(origin, lambda copy: copy.wait_send())
-        ),
-    )
-
-    def left(step):
-        for half in range(2):
-            for side in range(2):
-                x_ring(side, step, half, z).wait_send()
-                h_ring(side, step, half, z).wait_send()
-
-    loop(1, half_ring, left)
-    for side in range(2):
-        x_ring(side, half_ring, side, z).wait_send()
-        h_ring(side, half_ring, side, z).wait_send()
-
-    def handed(offset):
-        for half in range(2):
-            x_hand(offset, half, core).wait_send()
-            h_hand(offset, half, core).wait_send()
-        p_copy(offset).wait_send()
-
-    loop(0, z_count, handed)
-
-    def summed(step):
-        for half in range(2):
-            for side in range(2):
-                r_copy(step, side, half, z).wait_send()
-
-    loop(0, z_count - 1, summed)
+    all_left(h_ring, h_hand)
 
 
 def fused(ep_count, tp_count, width, operands):

time: 126 us -> 126 us (level)
  no operation moved by 1% of the time
where the time goes in v6:
time: 126 us
  Pallas kernels  121 us (96%)
  other arithmetic  4.37 us (3%)
    pallas_call x1, Pallas kernels, fused(): pl.pallas_call(functools.partial(fused_kernel, ep_count, z_count), out_sh...  121 us
    convert_element_type x2, other arithmetic, body(): return (mixed.astype(jnp.bfloat16), moe_out.astype(jnp.bfloat16))  3.39 us

profile of v6, /device:TPU:27, one launch (start us, length us, event | category | flops | bytes accessed | tf_op | source)
XLA Modules:
  0.0 125.8 jit_solution(3696534405343238639)
XLA Ops:
  0.7 1.0 multiply_sine_fusion
  1.6 120.7 %fused.1 = (f32[1024,128]{1,0:T(8,128)}, f32[32,2048]{1,0:T(8,128)}) custom-call(f32[16,1024]{1,0:T(8,128)} %get-tuple-element.7.cosine_ref, f32[16,1024]{1,0:T(8,128)} %get-tuple-element.6.sine_ref, bf16[32,1024]{1,0:T(8,128)(2,1)} %bitcast.14, f32[1,512]{1,0:T(1,128)} %bitcast.18, f32[1,256]{1,0:T(1,128)} %bitcast.19, f32[1,2048]{1,0:T(1,128)} %bitcast.15, ...), custom_call_target="tpu_custom_call" | custom-call | tf_op jit(solution)/shard_map/fused/pallas_call | solution.py:712
  122.4 1.8 %convert_element_type.14 = bf16[1024,128]{1,0:T(8,128)(2,1)} convert(f32[1024,128]{1,0:T(8,128)} %get-tuple-element.4) | non-fusion elementwise | flops 131072 | bytes 786432 | tf_op jit(solution)/shard_map/convert_element_type | solution.py:822
  124.2 1.6 %convert_element_type.15 = bf16[32,2048]{1,0:T(8,128)(2,1)} convert(f32[32,2048]{1,0:T(8,128)} %get-tuple-element.5) | non-fusion elementwise | flops 65536 | bytes 393216 | tf_op jit(solution)/shard_map/convert_element_type | solution.py:822
  (2 shorter events, 0.0 us)
